TPU v7x, 256 devices: a whole 4x4x8 slice. The times are simulated.
256 devices in a mesh: dp: 4 (over y), kv: 32 (over z, x), tp: 2 (over core).
Axes of the slice: x: 4, y: 4, z: 8, core: 2. Of those that a mesh axis runs over, the one named last changes fastest.
Arguments:
- tokens: bfloat16 [1024, 4096], P('dp', ('kv', 'tp')), may hold values from -11.5 to 11.5, as said below
- gain_mix: float32 [4096], replicated, may hold values from 0.1 to 1.9
- gain_mlp: float32 [4096], replicated, may hold values from 0.1 to 1.9
- decay_rate: float32 [16], replicated, may hold values from 0.01 to 1
- w_query: bfloat16 [4096, 1024], P('kv', 'tp'), may hold values from -0.09375 to 0.09375
- w_key: bfloat16 [4096, 1024], P('kv', 'tp'), may hold values from -0.09375 to 0.09375
- w_value: bfloat16 [4096, 2048], P('kv', 'tp'), may hold values from -0.09375 to 0.09375
- w_gate: bfloat16 [4096, 2048], P('kv', 'tp'), may hold values from -0.09375 to 0.09375
- w_mix: bfloat16 [2048, 4096], P('tp', 'kv'), may hold values from -0.125 to 0.125
- w_up: bfloat16 [4096, 16384], P(None, ('kv', 'tp')), may hold values from -0.09375 to 0.09375
- w_down: bfloat16 [16384, 4096], P(('kv', 'tp')), may hold values from -0.125 to 0.125
- state: float32 [1024, 16, 64, 128], P(('dp', 'kv'), 'tp'), may hold values from -2 to 2
Outputs:
- result: bfloat16 [1024, 4096], P('dp', ('kv', 'tp'))
- new_state: float32 [1024, 16, 64, 128], P(('dp', 'kv'), 'tp')
Inputs may be any that keep to these rules, and one draw needn't show every extreme that they name: `tokens`: feature scales differ across the features.
All inputs are finite; a program needn't handle non-finite values.
Results may differ from a plain program's by a relative error of at most 0.02.
Values may be sent and summed in bfloat16 or wider, within the bound.
A program may use at most 64 MiB of HBM per device.

v0:
```python
import jax
import jax.numpy as jnp
from jax import lax
from jax.sharding import Mesh
from jax.sharding import PartitionSpec as P

KV = ("kv_0", "kv_1")
KV_TP = ("kv_0", "kv_1", "tp")
DP_KV = ("dp", "kv_0", "kv_1")


EPS = 1e-06


def laid_out(parts, dim):
    shape = list(parts.shape[1:])
    shape[dim] *= parts.shape[0]
    return jnp.moveaxis(parts, 0, dim).reshape(shape)


def sent_to_all(x, axis):
    peers = lax.axis_size(axis)
    return lax.all_to_all(jnp.broadcast_to(x[None], (peers, *x.shape)), axis, 0, 0, tiled=True)


def gathered_copies(x, axis, dim):
    return laid_out(sent_to_all(x, axis), dim)


def of_everyone(x, axis):
    everything = sent_to_all(x, axis)
    return jnp.sum(everything, axis=0)


def cut_along(x, dim, peers):
    shape = x.shape
    parts = x.reshape(*shape[:dim], peers, shape[dim] // peers, *shape[dim + 1 :])
    return jnp.moveaxis(parts, dim, 0)


def sum_at_owner(x, axis, dim):
    parts = cut_along(x, dim, lax.axis_size(axis))
    arrived = lax.all_to_all(parts, axis, split_axis=0, concat_axis=0, tiled=True)
    return arrived.astype(jnp.float32).sum(axis=0)


def of_everyone_2(x, axis):
    return sent_to_all(x, axis).astype(jnp.float32).sum(axis=0)


def whole_of(x, axes, dim):
    if not axes:
        return x
    nearer = lax.all_gather(x, axes[-1], axis=dim, tiled=True)
    return whole_of(nearer, axes[:-1], dim)


def per_device(
    tokens,
    gain_mix,
    gain_mlp,
    decay_rate,
    w_query,
    w_key,
    w_value,
    w_gate,
    w_mix,
    w_up,
    w_down,
    state,
):
    seq_count, head_count, key_width, value_width = state.shape
    both_cols = gathered_copies(tokens, "tp", 1)
    col_count = both_cols.shape[1]
    col_start = lax.axis_index(KV) * col_count
    model_width = col_count * lax.axis_size(KV)
    block_f = both_cols.astype(jnp.float32)
    squares = jnp.sum(block_f * block_f, axis=1)
    row_total = of_everyone(squares, KV)
    first_scale = lax.rsqrt(row_total / model_width + EPS)
    gain_cols = lax.dynamic_slice_in_dim(gain_mix, col_start, col_count)
    normed = (block_f * first_scale[:, None] * gain_cols[None, :]).astype(jnp.bfloat16)
    own_inputs = sum_at_owner(
        jnp.concatenate(
            [
                jnp.dot(normed, weight, preferred_element_type=jnp.float32)
                for weight in (w_query, w_key, w_value, w_gate)
            ],
            axis=1,
        ).astype(jnp.bfloat16),
        KV,
        0,
    ).astype(jnp.bfloat16)
    query_end = head_count * key_width
    key_end = 2 * query_end
    value_end = key_end + head_count * value_width
    query_heads = (
        own_inputs[:, :query_end].astype(jnp.float32).reshape(seq_count, head_count, key_width)
    )
    key_heads = (
        own_inputs[:, query_end:key_end]
        .astype(jnp.float32)
        .reshape(seq_count, head_count, key_width)
    )
    key_heads = key_heads * key_width ** (-0.5)
    value_heads = (
        own_inputs[:, key_end:value_end]
        .astype(jnp.float32)
        .reshape(seq_count, head_count, value_width)
    )
    gate_heads = (
        own_inputs[:, value_end:].astype(jnp.float32).reshape(seq_count, head_count, value_width)
    )
    rates = lax.dynamic_slice_in_dim(decay_rate, lax.axis_index("tp") * head_count, head_count)
    decay = jnp.exp(-rates)[None, :, None, None]
    new_state = decay * state + key_heads[:, :, :, None] * value_heads[:, :, None, :]
    read = jnp.einsum("bhd,bhde->bhe", query_heads, new_state, precision=lax.Precision.HIGHEST)
    read = read * lax.rsqrt(jnp.mean(read * read, axis=2, keepdims=True) + EPS)
    heads_out = (
        (jax.nn.silu(gate_heads) * read)
        .reshape(seq_count, head_count * value_width)
        .astype(jnp.bfloat16)
    )
    partial_value = jnp.dot(
        gathered_copies(heads_out, KV, 0), w_mix, preferred_element_type=jnp.float32
    )
    rounded = lax.optimization_barrier(partial_value.astype(jnp.bfloat16)).astype(jnp.float32)
    mixed = of_everyone_2(rounded.astype(jnp.bfloat16), "tp").astype(jnp.float32)
    resid_block = (block_f + mixed).astype(jnp.bfloat16)
    rows_full = whole_of(resid_block, KV, 1)
    rows_f = rows_full.astype(jnp.float32)
    second_scale = lax.rsqrt(jnp.mean(rows_f * rows_f, axis=1, keepdims=True) + EPS)
    normed_mlp = (rows_f * second_scale * gain_mlp[None, :]).astype(jnp.bfloat16)
    upper = jnp.dot(normed_mlp, w_up, preferred_element_type=jnp.float32)
    hidden = jnp.square(jax.nn.relu(upper)).astype(jnp.bfloat16)
    summed = sum_at_owner(
        jnp.dot(hidden, w_down, preferred_element_type=jnp.float32).astype(jnp.bfloat16), KV_TP, 1
    )
    own_width = tokens.shape[1]
    residual_cols = lax.dynamic_slice_in_dim(
        rows_f, lax.axis_index(KV_TP) * own_width, own_width, 1
    )
    result = (residual_cols + summed).astype(jnp.bfloat16)
    return (result, new_state)


def solution(mesh):
    torus = Mesh(
        mesh.devices.reshape(mesh.shape["dp"], 8, 4, mesh.shape["tp"]), ("dp", "kv_0", "kv_1", "tp")
    )
    return jax.shard_map(
        per_device,
        mesh=torus,
        in_specs=(
            P("dp", KV_TP),
            P(),
            P(),
            P(),
            P(KV, "tp"),
            P(KV, "tp"),
            P(KV, "tp"),
            P(KV, "tp"),
            P("tp", KV),
            P(None, KV_TP),
            P(KV_TP, None),
            P(DP_KV, "tp", None, None),
        ),
        out_specs=(P("dp", KV_TP), P(DP_KV, "tp", None, None)),
        check_vma=False,
    )
```

profile of v0, /device:TPU:1, one launch (start us, length us, event | category | flops | bytes accessed | tf_op | source)
XLA Modules:
  0.0 245.8 jit_solution(14415253915606332065)
XLA Ops:
  7.2 0.0 copy-start
  7.2 0.9 broadcast_in_dim.8
  8.1 6.6 %all_to_all.31 = bf16[2,256,64]{1,2,0:T(8,128)(2,1)S(1)} all-to-all(bf16[2,256,64]{1,2,0:T(8,128)(2,1)S(1)} %broadcast_in_dim.8), channel_id=1, replica_groups=mesh['dp'=4,'kv_0'=8,'kv_1'=4,'tp'=2] {'tp'}, dimensions={0} | all-to-all | bytes 131072 | tf_op jit(solution)/shard_map/all_to_all | solution.py:23
  14.8 0.6 broadcast_in_dim.9
  15.4 9.3 %all-to-all-start.1 = ((f32[32,1,256]{2,1,0:T(1,128)}), f32[32,1,256]{2,1,0:T(1,128)S(1)}, u32[]{:S(2)}, u32[]{:S(2)}) async-start(f32[32,1,256]{2,1,0:T(1,128)} %broadcast_in_dim.9), calls=%async_computation.1 | async-start | bytes 65536 | tf_op jit(solution)/shard_map/all_to_all | solution.py:23
  24.8 0.1 copy.28
  25.0 0.2 reshape.129
  25.1 0.8 dynamic_slice.9
  25.9 7.6 %all-to-all-done.1 = f32[32,1,256]{2,1,0:T(1,128)S(1)} async-done(((f32[32,1,256]{2,1,0:T(1,128)}), f32[32,1,256]{2,1,0:T(1,128)S(1)}, u32[]{:S(2)}, u32[]{:S(2)}) %all-to-all-start.1) | async-done | bytes 32800 | tf_op jit(solution)/shard_map/all_to_all | solution.py:23
  33.5 0.1 reduce_sum.67
  33.5 0.1 rsqrt.28
  33.6 0.1 multiply_convert_fusion.10
  33.7 1.1 convolution_convert_fusion.3
  34.9 0.2 convolution_convert_fusion.4
  35.1 0.3 convolution_convert_fusion.1
  35.4 0.3 convolution_convert_fusion.2
  35.7 1.3 pad_maximum_fusion
  37.0 4.8 %all-to-all-start.2 = ((bf16[32,8,3072]{2,1,0:T(8,128)(2,1)}), bf16[32,8,3072]{2,1,0:T(8,128)(2,1)}, u32[]{:S(2)}, u32[]{:S(2)}) async-start(bf16[32,8,3072]{2,1,0:T(8,128)(2,1)} %pad_maximum_fusion), calls=%async_computation.2 | async-start | bytes 3145728 | tf_op jit(solution)/shard_map/all_to_all | solution.py:43
  41.8 0.1 negate_exponential_fusion
  41.9 36.0 %all-to-all-done.2 = bf16[32,8,3072]{2,1,0:T(8,128)(2,1)} async-done(((bf16[32,8,3072]{2,1,0:T(8,128)(2,1)}), bf16[32,8,3072]{2,1,0:T(8,128)(2,1)}, u32[]{:S(2)}, u32[]{:S(2)}) %all-to-all-start.2) | async-done | bytes 1572896 | tf_op jit(solution)/shard_map/all_to_all | solution.py:43
  77.9 1.6 reduce_sum.68
  79.5 0.1 mul.136
  79.6 0.1 reshape.140
  79.7 2.0 multiply_add_fusion
  81.7 1.3 copy-done.1
  83.0 1.1 fusion.21
  84.1 0.1 fusion.17
  84.2 0.1 fusion.19
  84.3 0.9 broadcast_in_dim.10
  85.1 7.3 %all-to-all-start.3 = ((bf16[32,8,1024]{2,1,0:T(8,128)(2,1)}), bf16[32,8,1024]{2,1,0:T(8,128)(2,1)S(1)}, u32[]{:S(2)}, u32[]{:S(2)}) async-start(bf16[32,8,1024]{2,1,0:T(8,128)(2,1)} %broadcast_in_dim.10), calls=%async_computation.3 | async-start | bytes 1048576 | tf_op jit(solution)/shard_map/all_to_all | solution.py:23
  92.4 0.0 all-gather.2.cloned.1.call-start
  92.4 0.1 copy.30
  92.5 14.4 %all-to-all-done.3 = bf16[32,8,1024]{2,1,0:T(8,128)(2,1)S(1)} async-done(((bf16[32,8,1024]{2,1,0:T(8,128)(2,1)}), bf16[32,8,1024]{2,1,0:T(8,128)(2,1)S(1)}, u32[]{:S(2)}, u32[]{:S(2)}) %all-to-all-start.3) | async-done | bytes 524320 | tf_op jit(solution)/shard_map/all_to_all | solution.py:23
  107.0 0.3 convolution_convert_fusion.5
  107.3 7.8 %all_to_all.32 = bf16[2,256,128]{2,1,0:T(8,128)(2,1)S(1)} all-to-all(bf16[2,256,128]{2,1,0:T(8,128)(2,1)S(1)} %broadcast_in_dim.11), channel_id=1, replica_groups=mesh['dp'=4,'kv_0'=8,'kv_1'=4,'tp'=2] {'tp'}, dimensions={0} | all-to-all | bytes 262144 | tf_op jit(solution)/shard_map/all_to_all | solution.py:23
  115.1 9.3 %all_gather.6 = bf16[256,512]{1,0:T(8,128)(2,1)} all-gather(bf16[256,128]{1,0:T(8,128)(2,1)S(1)} %add_convert_fusion.1), channel_id=1, replica_groups=mesh['dp'=4,'kv_0'=8,'kv_1'=4,'tp'=2] {'kv_1'}, dimensions={1}, use_global_device_ids=true | all-gather | bytes 327680 | tf_op jit(solution)/shard_map/all_gather | solution.py:54
  124.4 0.0 all-gather.2.cloned.1.call-update
  124.5 36.7 %all-gather.2.cloned.1.call-done = bf16[256,4096]{1,0:T(8,128)(2,1)} async-done(((bf16[256,512]{1,0:T(8,128)(2,1)}), bf16[256,4096]{1,0:T(8,128)(2,1)}) %all-gather.2.cloned.1.call-update) | async-done | bytes 2097168 | tf_op jit(solution)/shard_map/all_gather | solution.py:54
  161.1 2.1 multiply_reduce_fusion
  163.2 6.0 %convolution_convert_fusion = bf16[256,4096]{1,0:T(8,128)(2,1)} fusion(bf16[256,4096]{1,0:T(8,128)(2,1)S(1)} %copy-done, bf16[4096,256]{1,0:T(8,128)(2,1)} %param.21, f32[4096]{0:T(1024)S(1)} %copy-done.6, f32[256]{0:T(256)S(1)} %add_rsqrt_fusion.1, bf16[256,4096]{1,0:T(8,128)(2,1)} %all-gather.2.cloned.1.call-done), kind=kOutput, calls=%fused_computation | convolution fusion | flops 1079181312 | bytes 8406016 | tf_op jit(solution)/shard_map/dot_general | solution.py:137
  169.2 4.1 %copy.31 = bf16[256,4096]{0,1:T(8,128)(2,1)} copy(bf16[256,4096]{1,0:T(8,128)(2,1)} %convolution_convert_fusion) | data formatting | bytes 4194304 | tf_op jit(solution)/shard_map/convert_element_type | solution.py:137
  173.3 12.3 %all-to-all-start.5 = ((bf16[64,256,64]{1,2,0:T(8,128)(2,1)}), bf16[64,256,64]{1,2,0:T(8,128)(2,1)}, u32[]{:S(2)}, u32[]{:S(2)}) async-start(bf16[64,256,64]{1,2,0:T(8,128)(2,1)} %bitcast.56), calls=%async_computation.5 | async-start | bytes 4194304 | tf_op jit(solution)/shard_map/all_to_all | solution.py:43
  185.6 4.0 %convert_element_type.92 = f32[256,4096]{1,0:T(8,128)} convert(bf16[256,4096]{1,0:T(8,128)(2,1)} %all-gather.2.cloned.1.call-done) | non-fusion elementwise | flops 1048576 | bytes 6291456 | tf_op jit(solution)/shard_map/convert_element_type | solution.py:131
  189.6 45.6 %all-to-all-done.5 = bf16[64,256,64]{1,2,0:T(8,128)(2,1)} async-done(((bf16[64,256,64]{1,2,0:T(8,128)(2,1)}), bf16[64,256,64]{1,2,0:T(8,128)(2,1)}, u32[]{:S(2)}, u32[]{:S(2)}) %all-to-all-start.5) | async-done | bytes 2097184 | tf_op jit(solution)/shard_map/all_to_all | solution.py:43
  235.2 1.9 convert_reduce_fusion
  237.1 0.1 copy.32
  237.2 1.0 add_convert_fusion
  238.2 0.7 copy.33
  (26 shorter events, 0.2 us)
Async XLA Ops:
  7.2 156.0 %copy-start = (bf16[256,4096]{1,0:T(8,128)(2,1)S(1)}, bf16[256,4096]{1,0:T(8,128)(2,1)}, u32[]{:S(2)}) copy-start(bf16[256,4096]{1,0:T(8,128)(2,1)} %param.22) | copy-start | bytes 6291460
  7.2 27.7 %copy-start.5 = (bf16[128,512]{1,0:T(8,128)(2,1)S(1)}, bf16[128,512]{1,0:T(8,128)(2,1)}, u32[]{:S(2)}) copy-start(bf16[128,512]{1,0:T(8,128)(2,1)} %param.16) | copy-start | bytes 393220
  7.2 27.9 %copy-start.2 = (bf16[128,1024]{1,0:T(8,128)(2,1)S(1)}, bf16[128,1024]{1,0:T(8,128)(2,1)}, u32[]{:S(2)}) copy-start(bf16[128,1024]{1,0:T(8,128)(2,1)} %param.19) | copy-start | bytes 786436
  7.2 28.2 %copy-start.3 = (bf16[128,1024]{1,0:T(8,128)(2,1)S(1)}, bf16[128,1024]{1,0:T(8,128)(2,1)}, u32[]{:S(2)}) copy-start(bf16[128,1024]{1,0:T(8,128)(2,1)} %param.18) | copy-start | bytes 786436
  15.4 18.0 %all-to-all-start.1 = ((f32[32,1,256]{2,1,0:T(1,128)}), f32[32,1,256]{2,1,0:T(1,128)S(1)}, u32[]{:S(2)}, u32[]{:S(2)}) async-start(f32[32,1,256]{2,1,0:T(1,128)} %broadcast_in_dim.9), calls=%async_computation.1 | async-start | bytes 65536 | tf_op jit(solution)/shard_map/all_to_all | solution.py:23
  37.0 4.9 %copy-start.7 = (f32[16]{0:T(128)S(1)}, f32[16]{0:T(128)}, u32[]{:S(2)}) copy-start(f32[16]{0:T(128)} %param.15) | copy-start | bytes 196
  37.0 40.9 %all-to-all-start.2 = ((bf16[32,8,3072]{2,1,0:T(8,128)(2,1)}), bf16[32,8,3072]{2,1,0:T(8,128)(2,1)}, u32[]{:S(2)}, u32[]{:S(2)}) async-start(bf16[32,8,3072]{2,1,0:T(8,128)(2,1)} %pad_maximum_fusion), calls=%async_computation.2 | async-start | bytes 3145728 | tf_op jit(solution)/shard_map/all_to_all | solution.py:43
  81.7 1.3 copy-start.1
  83.0 24.0 %copy-start.4 = (bf16[1024,128]{1,0:T(8,128)(2,1)S(1)}, bf16[1024,128]{1,0:T(8,128)(2,1)}, u32[]{:S(2)}) copy-start(bf16[1024,128]{1,0:T(8,128)(2,1)} %param.20) | copy-start | bytes 786436
  85.1 21.9 %all-to-all-start.3 = ((bf16[32,8,1024]{2,1,0:T(8,128)(2,1)}), bf16[32,8,1024]{2,1,0:T(8,128)(2,1)S(1)}, u32[]{:S(2)}, u32[]{:S(2)}) async-start(bf16[32,8,1024]{2,1,0:T(8,128)(2,1)} %broadcast_in_dim.10), calls=%async_computation.3 | async-start | bytes 1048576 | tf_op jit(solution)/shard_map/all_to_all | solution.py:23
  92.4 68.7 %all-gather.2.cloned.1.call-start = ((), (), s32[]{:S(2)}) async-start(), calls=%async_computation.6 | async-start | bytes 2359296 | tf_op jit(solution)/shard_map/all_gather | solution.py:54
  92.5 70.7 %copy-start.6 = (f32[4096]{0:T(1024)S(1)}, f32[4096]{0:T(1024)}, u32[]{:S(2)}) copy-start(f32[4096]{0:T(1024)} %param.14) | copy-start | bytes 49156
  173.3 61.9 %all-to-all-start.5 = ((bf16[64,256,64]{1,2,0:T(8,128)(2,1)}), bf16[64,256,64]{1,2,0:T(8,128)(2,1)}, u32[]{:S(2)}, u32[]{:S(2)}) async-start(bf16[64,256,64]{1,2,0:T(8,128)(2,1)} %bitcast.56), calls=%async_computation.5 | async-start | bytes 4194304 | tf_op jit(solution)/shard_map/all_to_all | solution.py:43
Sparse Core Ops, SparseCore 0:
  124.6 36.4 all-gather.1
where the time goes:
time: 247 us; the launch traced here: 246 us
  waiting for transfers between devices  140 us (57%)
  starting transfers between devices  33.8 us (14%)
  blocking collectives  23.7 us (10%)
  other arithmetic  14.4 us (6%)
  between operations  14.3 us (6%)
  local copies, waits for them, and re-layouts  10.1 us (4%)
  matrix products  9.24 us (4%)
    all_to_all x2, waiting for transfers between devices, sum_at_owner(): lax.all_to_all(parts, axis, split_axis=0, concat_axis=0, tiled=True)  81.6 us
    all_gather x1, waiting for transfers between devices, whole_of(): nearer = lax.all_gather(x, axes[-1], axis=dim, tiled=True)  36.7 us
    all_to_all x2, waiting for transfers between devices, sent_to_all(): lax.all_to_all(jnp.broadcast_to(x[None], (peers, *x.shape)), axis, 0, 0,...  22 us
    all_to_all x2, starting transfers between devices, sum_at_owner(): lax.all_to_all(parts, axis, split_axis=0, concat_axis=0, tiled=True)  17.1 us
    all_to_all x2, starting transfers between devices, sent_to_all(): lax.all_to_all(jnp.broadcast_to(x[None], (peers, *x.shape)), axis, 0, 0,...  16.6 us
    all_to_all x2, blocking collectives, sent_to_all(): lax.all_to_all(jnp.broadcast_to(x[None], (peers, *x.shape)), axis, 0, 0,...  14.4 us
    all_gather x1, blocking collectives, whole_of(): nearer = lax.all_gather(x, axes[-1], axis=dim, tiled=True)  9.3 us
    dot_general x1, matrix products, per_device(): jnp.dot(hidden, w_down, preferred_element_type=jnp.float32)  5.99 us
  transfers between devices with their start and end apart: 5, of which 5 were waited for; matrix products, arithmetic and copies ran while one was open for 2% of the time, Pallas kernels for 0%

commit v1 on v0

v1 whole, which is shorter than its diff:
```python
import jax
import jax.numpy as jnp
from jax import lax
from jax.sharding import Mesh
from jax.sharding import PartitionSpec as P
from jax.experimental import pallas as pl
from jax.experimental.pallas import tpu as pltpu

KV = ("kv_0", "kv_1")
KV_TP = ("kv_0", "kv_1", "tp")
DP_KV = ("dp", "kv_0", "kv_1")
EPS = 1e-06
F32 = jnp.float32
BF16 = jnp.bfloat16
MESH = pl.DeviceIdType.MESH
NZ = 8
NX = 4
FAR = (4, 3, 5, 2, 6, 1, 7)


def kernel(
    tokens, gain_mix, gain_mlp, rates, w_query, w_key, w_value, w_gate, w_mix, w_up, w_down, state,
    out, new_state,
    pack, tok_in, tokf, wbuf, wm, wup, wdn, st,
    sbuf, rbuf, ssq_s, ssq_r, rdbuf, hall, pbuf, pin, rg,
    xsb, xrb, zsb, zrb, fsend, frecv, fin,
    loc_sem, ns_sem, tok_ss, tok_rs, w_ss, w_rs, mix_ss, mix_rs, mlp_ss, mlp_rs,
    p1_ss, p1_rs, ssq_ss, ssq_rs, h_ss, h_rs, pr_ss, pr_rs,
    rz_ss, rz_rs, rx_ss, rx_rs, xs_ss, xs_rs, zs_ss, zs_rs, f_ss, f_rs,
):
    z = lax.axis_index("kv_0")
    x = lax.axis_index("kv_1")
    c = lax.axis_index("tp")
    kv = z * NX + x

    def zp(d):
        return lax.rem(z + d, NZ)

    def xp(d):
        return lax.rem(x + d, NX)

    bar = pltpu.get_barrier_semaphore()

    def greet(i, _):
        pl.semaphore_signal(
            bar, inc=1, device_id={"kv_0": zp(i // NX), "kv_1": xp(i % NX)}, device_id_type=MESH
        )
        return 0

    lax.fori_loop(1, NZ * NX, greet, 0)
    for dx in range(NX):
        pl.semaphore_signal(bar, inc=1, device_id={"kv_1": xp(dx), "tp": 1 - c}, device_id_type=MESH)

    def local(src, dst, i):
        cp = pltpu.make_async_copy(src, dst, loc_sem.at[i])
        cp.start()
        return cp

    cq = pl.ds(pl.multiple_of(x * 128, 128), 128)
    cv = pl.ds(pl.multiple_of(x * 256, 256), 256)
    ld_w = [
        local(w_query.at[:, cq], wbuf.at[x, :, 0:128], 0),
        local(w_key.at[:, cq], wbuf.at[x, :, 128:256], 1),
        local(w_value.at[:, cv], wbuf.at[x, :, 256:512], 2),
        local(w_gate.at[:, cv], wbuf.at[x, :, 512:768], 3),
    ]
    ld_st = local(state, st, 4)
    ld_mix = local(w_mix, wm.at[x], 5)
    ld_up = local(w_up, wup.at[c], 6)
    ld_dn = local(w_down, wdn.at[c], 7)

    t32 = tokens[...].astype(F32)
    packed = jnp.concatenate([t32[:128], t32[128:]], axis=1).astype(BF16)
    tok_in[x, c] = packed

    pl.semaphore_wait(bar, 35)

    def remote(src, dst, ss, rs, dev):
        cp = pltpu.make_async_remote_copy(
            src_ref=src, dst_ref=dst, send_sem=ss, recv_sem=rs, device_id=dev, device_id_type=MESH
        )
        cp.start()
        return cp

    tok_cp = []
    for i, (dx, other) in enumerate([(2, 0), (2, 1), (1, 0), (3, 0), (1, 1), (3, 1), (0, 1)]):
        dev = {"kv_1": xp(dx), "tp": (1 - c) if other else c}
        tok_cp.append(remote(tok_in.at[x, c], tok_in.at[x, c], tok_ss.at[i], tok_rs.at[i], dev))

    w_cp = {0: [], 1: [], 2: []}
    for dx in (2, 1, 3):
        dev = {"kv_1": xp(dx)}
        dq = pl.ds(pl.multiple_of(xp(dx) * 128, 128), 128)
        w_cp[0].append(remote(w_query.at[:, dq], wbuf.at[x, :, 0:128], w_ss.at[0, dx], w_rs.at[0, dx], dev))
        w_cp[0].append(remote(w_key.at[:, dq], wbuf.at[x, :, 128:256], w_ss.at[1, dx], w_rs.at[1, dx], dev))
    for j, (w, lo) in enumerate(((w_value, 256), (w_gate, 512))):
        for dx in (2, 1, 3):
            dev = {"kv_1": xp(dx)}
            dv = pl.ds(pl.multiple_of(xp(dx) * 256, 256), 256)
            w_cp[j + 1].append(
                remote(w.at[:, dv], wbuf.at[x, :, lo:lo + 256], w_ss.at[2 + j, dx], w_rs.at[2 + j, dx], dev)
            )

    partner = {"tp": 1 - c}
    mlp_cp = [
        remote(w_up, wup.at[c], mlp_ss.at[0], mlp_rs.at[0], partner),
        remote(w_down, wdn.at[c], mlp_ss.at[1], mlp_rs.at[1], partner),
    ]

    for cp in tok_cp:
        cp.wait_recv()
    low = lax.broadcasted_iota(jnp.int32, (128, 128), 1) < 64
    squares = jnp.zeros((256, 128), F32)
    for xx in range(NX):
        a = tok_in[xx, 0].astype(F32)
        b = tok_in[xx, 1].astype(F32)
        top = jnp.where(low, a, pltpu.roll(b, 64, 1))
        bottom = jnp.where(low, pltpu.roll(a, 64, 1), b)
        both = jnp.concatenate([top, bottom], axis=0)
        tokf[:, :, xx * 128:(xx + 1) * 128] = both.reshape(32, 8, 128)
        squares = squares + both * both
    ssq_s[...] = jnp.broadcast_to(jnp.sum(squares, axis=1, keepdims=True), (256, 128)).reshape(32, 8, 128)
    ssq_cp = []
    for dz in FAR:
        ssq_cp.append(
            remote(ssq_s.at[zp(dz) * NX + x], ssq_r.at[dz], ssq_ss.at[dz], ssq_rs.at[dz], {"kv_0": zp(dz)})
        )
    fz = pl.ds(pl.multiple_of(z * 512, 512), 512)
    normed = (tokf[...].reshape(256, 512) * gain_mix[:, fz]).astype(BF16)

    for ch in range(3):
        for cp in w_cp[ch]:
            cp.wait_recv()
        for ld in (ld_w[0:2], ld_w[2:3], ld_w[3:4])[ch]:
            ld.wait()
        wch = wbuf[:, :, ch * 256:(ch + 1) * 256].reshape(512, 256)
        part = jnp.dot(normed, wch, preferred_element_type=F32).reshape(32, 8, 256)
        sbuf[ch] = jnp.concatenate([part[:, :, :128], part[:, :, 128:]], axis=1).astype(BF16)

        def scatter(i, _, ch=ch):
            zz, xx = zp(i // NX), xp(i % NX)
            remote(
                sbuf.at[ch, zz * NX + xx], rbuf.at[ch, i], p1_ss.at[ch], p1_rs.at[ch], {"kv_0": zz, "kv_1": xx}
            )
            return 0

        lax.fori_loop(1, NZ * NX, scatter, 0)

    mix_cp = []
    for dx in (2, 1, 3):
        mix_cp.append(remote(w_mix, wm.at[x], mix_ss.at[dx], mix_rs.at[dx], {"kv_1": xp(dx)}))

    for cp in ssq_cp:
        cp.wait_recv()
    ssq_r[0] = ssq_s[kv]
    total = jnp.sum(ssq_r[...], axis=0)
    first_scale = lax.rsqrt(total / 4096.0 + EPS)
    scale16 = jnp.concatenate([first_scale, first_scale], axis=0)[None]

    def own(ch):
        pltpu.make_async_copy(rbuf.at[ch, 1:32], rbuf.at[ch, 1:32], p1_rs.at[ch]).wait()
        rbuf[ch, 0] = sbuf[ch, kv]
        summed = jnp.sum(rbuf[ch].astype(F32).reshape(NZ, NX, 16, 128), axis=0)
        return (summed * scale16).astype(BF16).astype(F32)

    qk = own(0)
    qs = qk[:, :8].reshape(32, 128)
    ks = qk[:, 8:].reshape(32, 128) * 0.125
    turned = jnp.transpose(jnp.concatenate([qs, ks, jnp.zeros((64, 128), F32)], axis=0))
    vals = own(1)
    ld_st.wait()
    ns_cp = []
    decays = []
    for dx in range(NX):
        xs = xp(NX - dx)
        pair = []
        for hh in range(2):
            rate = rates[c * 8 + xs * 2 + hh]
            pair.append(jnp.exp(-jnp.full((1, 128), rate, F32)))
        decays.append(pair)
    for b in range(8):
        for dx in range(NX):
            xs = xp(NX - dx)
            for hh in range(2):
                rows = slice(hh * 64, (hh + 1) * 64)
                col = dx * 8 + b
                old = st[b, xs, rows, :]
                new = decays[dx][hh] * old + turned[rows, 32 + col:33 + col] * vals[dx, hh * 8 + b:hh * 8 + b + 1, :]
                st[b, xs, rows, :] = new
                rdbuf[dx, hh * 8 + b:hh * 8 + b + 1, :] = jnp.sum(
                    turned[rows, col:col + 1] * new, axis=0, keepdims=True
                )
        cp = pltpu.make_async_copy(st.at[b], new_state.at[b], ns_sem.at[b])
        cp.start()
        ns_cp.append(cp)
    gates = own(2)
    read = rdbuf[...]
    read = read * lax.rsqrt(jnp.mean(read * read, axis=2, keepdims=True) + EPS)
    heads = (gates / (1.0 + jnp.exp(-gates)) * read).astype(BF16)
    for dx in range(NX):
        hall[z, xp(NX - dx)] = heads[dx]
    h_cp = []
    for dz in FAR:
        h_cp.append(remote(hall.at[z], hall.at[z], h_ss.at[dz], h_rs.at[dz], {"kv_0": zp(dz)}))
    for cp in h_cp:
        cp.wait_recv()
    for cp in mix_cp:
        cp.wait_recv()
    ld_mix.wait()

    pieces = []
    for xs in range(NX):
        both = hall[:, xs].astype(F32)
        for hh in range(2):
            pieces.append(both[:, hh * 8:(hh + 1) * 8].reshape(64, 128).astype(BF16))
    lhs = jnp.concatenate(pieces, axis=1)
    for xx in range(NX):
        prod = jnp.dot(lhs, wm[xx], preferred_element_type=F32).astype(BF16)
        pbuf[0, :, xx * 128:(xx + 1) * 128] = prod[:32]
        pbuf[1, :, xx * 128:(xx + 1) * 128] = prod[32:]
    pr_cp = remote(pbuf.at[1 - c], pin, pr_ss, pr_rs, partner)
    pr_cp.wait_recv()
    mixed = pbuf[c].astype(F32) + pin[...].astype(F32)
    own_tok = []
    for zl in range(4):
        own_tok.append(tokf[(c * 4 + zl) * NX + x])
    rg[x, z] = (jnp.concatenate(own_tok, axis=0) + mixed).astype(BF16)

    rz_cp = {}
    for dz in FAR:
        rz_cp[dz] = remote(rg.at[x, z], rg.at[x, z], rz_ss.at[dz], rz_rs.at[dz], {"kv_0": zp(dz)})
    rx_cp = []
    ORDER = (0, 1, 7, 2, 6, 3, 5, 4)
    for dz in ORDER:
        zz = lax.rem(z - dz + NZ, NZ)
        if dz:
            rz_cp[dz].wait_recv()
        for dx in (2, 1, 3):
            rx_cp.append(
                remote(rg.at[x, zz], rg.at[x, zz], rx_ss.at[dz, dx], rx_rs.at[dz, dx], {"kv_1": xp(dx)})
            )
    ld_up.wait()
    mlp_cp[0].wait_recv()
    acc = [jnp.zeros((128, 256), F32), jnp.zeros((128, 256), F32)]
    squares = jnp.zeros((128, 128), F32)
    for i, dz in enumerate(ORDER):
        zz = lax.rem(z - dz + NZ, NZ)
        for k in range(3):
            rx_cp[i * 3 + k].wait_recv()
        rows = rg[:, zz].reshape(128, 512).astype(F32)
        fk = pl.ds(pl.multiple_of(zz * 512, 512), 512)
        for q in range(4):
            piece = rows[:, q * 128:(q + 1) * 128]
            squares = squares + piece * piece
        lhs = (rows * gain_mlp[:, fk]).astype(BF16)
        for cc in range(2):
            acc[cc] = acc[cc] + jnp.dot(lhs, wup[cc, fk, :], preferred_element_type=F32)
    second_scale = lax.rsqrt(jnp.sum(squares, axis=1, keepdims=True) / 4096.0 + EPS)
    hid = []
    for cc in range(2):
        upper = jnp.maximum(acc[cc] * second_scale, 0.0)
        hid.append((upper * upper).astype(BF16))

    ld_dn.wait()
    mlp_cp[1].wait_recv()
    xs_cp = {}
    for i in range(NZ):
        dz = (FAR + (0,))[i]
        zz = zp(dz)
        fk = pl.ds(pl.multiple_of(zz * 512, 512), 512)
        part = jnp.dot(hid[0], wdn[0, :, fk], preferred_element_type=F32)
        part = part + jnp.dot(hid[1], wdn[1, :, fk], preferred_element_type=F32)
        part = part.astype(BF16)
        for xx in range(NX):
            xsb[dz, xx] = part[:, xx * 128:(xx + 1) * 128]
        for dx in (2, 1, 3):
            xs_cp[dz, dx] = remote(
                xsb.at[dz, xp(dx)], xrb.at[dz, dx - 1], xs_ss.at[dz, dx], xs_rs.at[dz, dx], {"kv_1": xp(dx)}
            )
    zs_cp = {}
    own_sum = None
    for i in range(NZ):
        dz = (FAR + (0,))[i]
        for dx in (2, 1, 3):
            xs_cp[dz, dx].wait_recv()
        summed = xsb[dz, x].astype(F32) + jnp.sum(xrb[dz].astype(F32), axis=0)
        if dz:
            zsb[dz] = summed.astype(BF16)
            zs_cp[dz] = remote(zsb.at[dz], zrb.at[dz - 1], zs_ss.at[dz], zs_rs.at[dz], {"kv_0": zp(dz)})
        else:
            own_sum = summed
    for dz in FAR:
        zs_cp[dz].wait_recv()
    down = own_sum + jnp.sum(zrb[...].astype(F32), axis=0)
    lanes = pl.ds(pl.multiple_of(x * 128, 128), 128)
    res = rg[:, z, :, lanes].reshape(128, 128).astype(F32)
    fsend[...] = (res + down).astype(BF16)
    f_cp = remote(fsend, frecv, f_ss, f_rs, partner)
    f_cp.wait_recv()
    for who, ref in ((c, fsend), (1 - c, frecv)):
        block = ref[...].astype(F32)
        for xs in range(NX):
            for zl in range(4):
                r0 = xs * 32 + zl * 8
                fin[(who * 4 + zl) * NX + xs] = block[r0:r0 + 8]
    done = fin[...].reshape(256, 128)
    out[...] = jnp.where(c == 0, done, pltpu.roll(done, 64, 1))[:, :64].astype(BF16)

    for cp in tok_cp + w_cp[0] + w_cp[1] + w_cp[2] + mlp_cp + ssq_cp + mix_cp + h_cp + [pr_cp]:
        cp.wait_send()
    for ch in range(3):
        pltpu.make_async_copy(sbuf.at[ch, 1:32], sbuf.at[ch, 1:32], p1_ss.at[ch]).wait()
    for cp in list(rz_cp.values()) + rx_cp + list(xs_cp.values()) + list(zs_cp.values()) + [f_cp]:
        cp.wait_send()
    for cp in ns_cp:
        cp.wait()


def per_device(
    tokens, gain_mix, gain_mlp, decay_rate, w_query, w_key, w_value, w_gate, w_mix, w_up, w_down, state
):
    vm = pl.BlockSpec(memory_space=pltpu.VMEM)
    hbm = pl.BlockSpec(memory_space=pltpu.HBM)
    dma = pltpu.SemaphoreType.DMA
    result, new_state = pl.pallas_call(
        kernel,
        out_shape=(
            jax.ShapeDtypeStruct((256, 64), BF16),
            jax.ShapeDtypeStruct((8, 4, 128, 128), F32),
        ),
        in_specs=[vm, vm, vm, pl.BlockSpec(memory_space=pltpu.SMEM)] + [hbm] * 8,
        out_specs=(vm, hbm),
        scratch_shapes=[
            pltpu.VMEM((128, 128), BF16),
            pltpu.VMEM((4, 2, 128, 128), BF16),
            pltpu.VMEM((32, 8, 512), F32),
            pltpu.VMEM((4, 128, 768), BF16),
            pltpu.VMEM((4, 1024, 128), BF16),
            pltpu.VMEM((2, 4096, 256), BF16),
            pltpu.VMEM((2, 256, 4096), BF16),
            pltpu.VMEM((8, 4, 128, 128), F32),
            pltpu.VMEM((3, 32, 16, 128), BF16),
            pltpu.VMEM((3, 32, 16, 128), BF16),
            pltpu.VMEM((32, 8, 128), F32),
            pltpu.VMEM((8, 8, 128), F32),
            pltpu.VMEM((4, 16, 128), F32),
            pltpu.VMEM((8, 4, 16, 128), BF16),
            pltpu.VMEM((2, 32, 512), BF16),
            pltpu.VMEM((32, 512), BF16),
            pltpu.VMEM((4, 8, 32, 512), BF16),
            pltpu.VMEM((8, 4, 128, 128), BF16),
            pltpu.VMEM((8, 3, 128, 128), BF16),
            pltpu.VMEM((8, 128, 128), BF16),
            pltpu.VMEM((7, 128, 128), BF16),
            pltpu.VMEM((128, 128), BF16),
            pltpu.VMEM((128, 128), BF16),
            pltpu.VMEM((32, 8, 128), F32),
            dma((8,)), dma((8,)), dma((7,)), dma((7,)), dma((4, 4)), dma((4, 4)), dma((4,)), dma((4,)),
            dma((2,)), dma((2,)), dma((3,)), dma((3,)), dma((8,)), dma((8,)), dma((8,)), dma((8,)),
            dma, dma, dma((8,)), dma((8,)), dma((8, 4)), dma((8, 4)), dma((8, 4)), dma((8, 4)),
            dma((8,)), dma((8,)), dma, dma,
        ],
        compiler_params=pltpu.CompilerParams(
            collective_id=0, has_side_effects=True, vmem_limit_bytes=60 * 1024 * 1024
        ),
        name="layer",
    )(
        tokens, gain_mix.reshape(1, 4096), gain_mlp.reshape(1, 4096), decay_rate,
        w_query, w_key, w_value, w_gate, w_mix, w_up, w_down, state.reshape(8, 4, 128, 128),
    )
    return result, new_state.reshape(8, 8, 64, 128)


def solution(mesh):
    torus = Mesh(
        mesh.devices.reshape(mesh.shape["dp"], 8, 4, mesh.shape["tp"]), ("dp", "kv_0", "kv_1", "tp")
    )
    return jax.shard_map(
        per_device,
        mesh=torus,
        in_specs=(
            P("dp", KV_TP),
            P(),
            P(),
            P(),
            P(KV, "tp"),
            P(KV, "tp"),
            P(KV, "tp"),
            P(KV, "tp"),
            P("tp", KV),
            P(None, KV_TP),
            P(KV_TP, None),
            P(DP_KV, "tp", None, None),
        ),
        out_specs=(P("dp", KV_TP), P(DP_KV, "tp", None, None)),
        check_vma=False,
    )
```

time: 247 us -> 89.7 us (0.36)
  waiting for transfers between devices: 140 us -> 0 us
  Pallas kernels: 0 us -> 82.6 us
  starting transfers between devices: 33.8 us -> 0 us
  blocking collectives: 23.7 us -> 0 us
  other arithmetic: 14.4 us -> 0 us
  between operations: 14.3 us -> 0.64 us
  matrix products: 9.24 us -> 0 us
  local copies, waits for them, and re-layouts: 10.1 us -> 6.19 us
    all_to_all x4 -> x0, waiting for transfers between devices: 104 us -> none  [the longest x2 81.6 us: sum_at_owner(): lax.all_to_all(parts, axis, split_axis=0, concat_axis=0, tiled=True)]
    pallas_call x0 -> x1, Pallas kernels: none -> 82.6 us  [per_device(): pl.pallas_call(kernel, out_shape=(jax.ShapeDtypeStruct((256, 64), BF16),...]
    all_gather x1 -> x0, waiting for transfers between devices: 36.7 us -> none  [whole_of(): nearer = lax.all_gather(x, axes[-1], axis=dim, tiled=True)]
    all_to_all x4 -> x0, starting transfers between devices: 33.7 us -> none  [the longest x2 17.1 us: sum_at_owner(): lax.all_to_all(parts, axis, split_axis=0, concat_axis=0, tiled=True)]
    all_to_all x2 -> x0, blocking collectives: 14.4 us -> none  [sent_to_all(): lax.all_to_all(jnp.broadcast_to(x[None], (peers, *x.shape)), axis, 0, 0,...]
    all_gather x1 -> x0, blocking collectives: 9.3 us -> none  [whole_of(): nearer = lax.all_gather(x, axes[-1], axis=dim, tiled=True)]
    dot_general x7 -> x0, matrix products: 9.24 us -> none  [the longest x1 5.99 us: per_device(): jnp.dot(hidden, w_down, preferred_element_type=jnp.float32)]
    reduce_sum x7 -> x0, other arithmetic: 5.81 us -> none  [the longest x2 3.53 us: sum_at_owner(): return arrived.astype(jnp.float32).sum(axis=0)]
  transfers between devices with their start and end apart: 5 -> 0, of which waited for: 5 -> 0; matrix products, arithmetic and copies ran while one was open for 2% -> 0% of each run, Pallas kernels for 0% -> 0%
where the time goes in v1:
time: 89.7 us; the launch traced here: 89.4 us
  Pallas kernels  82.6 us (92%)
  local copies, waits for them, and re-layouts  6.19 us (7%)
    pallas_call x1, Pallas kernels, per_device(): pl.pallas_call(kernel, out_shape=(jax.ShapeDtypeStruct((256, 64), BF16),...  82.6 us
    unnamed x3, local copies, waits for them, and re-layouts  6.19 us

profile of v1, /device:TPU:1, one launch (start us, length us, event | category | flops | bytes accessed | tf_op | source)
XLA Modules:
  0.0 89.4 jit_solution(11653475562186151966)
XLA Ops:
  0.6 1.5 %copy.14.tokens = bf16[256,64]{1,0:T(8,128)(2,1)} copy(bf16[256,64]{0,1:T(8,128)(2,1)} %param.12) | data formatting | bytes 65536 | tf_op args[0]
  2.1 82.6 %layer.1 = (bf16[256,64]{1,0:T(8,128)(2,1)}, f32[8,4,128,128]{3,2,1,0:T(8,128)}) custom-call(bf16[256,64]{1,0:T(8,128)(2,1)} %copy.14.tokens, f32[1,4096]{1,0:T(1,128)} %bitcast.6, f32[1,4096]{1,0:T(1,128)} %bitcast.7, f32[16]{0:T(128)} %rates.1, bf16[128,512]{1,0:T(8,128)(2,1)} %w_query.1, bf16[128,512]{1,0:T(8,128)(2,1)} %w_key.1, ...), custom_call_target="tpu_custom_call" | custom-call | tf_op jit(solution)/shard_map/layer/pallas_call | solution.py:325
  84.7 1.5 %copy.15 = bf16[256,64]{0,1:T(8,128)(2,1)} copy(bf16[256,64]{1,0:T(8,128)(2,1)} %get-tuple-element.6) | data formatting | bytes 65536
  86.2 3.2 %copy.17 = f32[8,8,64,128]{3,2,1,0:T(8,128)} copy(f32[8,8,64,128]{3,2,1,0:T(8,128)} %bitcast.4) | data formatting | bytes 4194304

commit v2 on v1

--- a/solution.py
+++ b/solution.py
@@ -19,18 +19,19 @@
 
 
 def kernel(
-    tokens, gain_mix, gain_mlp, rates, w_query, w_key, w_value, w_gate, w_mix, w_up, w_down, state,
-    out, new_state,
-    pack, tok_in, tokf, wbuf, wm, wup, wdn, st,
-    sbuf, rbuf, ssq_s, ssq_r, rdbuf, hall, pbuf, pin, rg,
-    xsb, xrb, zsb, zrb, fsend, frecv, fin,
-    loc_sem, ns_sem, tok_ss, tok_rs, w_ss, w_rs, mix_ss, mix_rs, mlp_ss, mlp_rs,
+    tokens, gain_mix_h, gain_mlp_h, rates, w_query, w_key, w_value, w_gate, w_mix, w_up, w_down, state,
+    out, keys_out, vals_out,
+    gain_mix, gain_mlp, tok_in, tokf, wbuf, wm, wup, wdn, st,
+    sbuf, rbuf, ssq_s, ssq_r, qk_abs, v_abs, g_abs, rdbuf, hall, pbuf, pin, rg,
+    xsb, xrb, zsb, zrb, fsend, frecv, fin, fint,
+    loc_sem, tok_ss, tok_rs, w_ss, w_rs, mix_ss, mix_rs, my_ss, my_rs, mlp_ss, mlp_rs,
     p1_ss, p1_rs, ssq_ss, ssq_rs, h_ss, h_rs, pr_ss, pr_rs,
     rz_ss, rz_rs, rx_ss, rx_rs, xs_ss, xs_rs, zs_ss, zs_rs, f_ss, f_rs,
 ):
     z = lax.axis_index("kv_0")
     x = lax.axis_index("kv_1")
     c = lax.axis_index("tp")
+    y = lax.axis_index("dp")
     kv = z * NX + x
 
     def zp(d):
@@ -50,6 +51,8 @@
     lax.fori_loop(1, NZ * NX, greet, 0)
     for dx in range(NX):
         pl.semaphore_signal(bar, inc=1, device_id={"kv_1": xp(dx), "tp": 1 - c}, device_id_type=MESH)
+    for dy in range(1, 4):
+        pl.semaphore_signal(bar, inc=1, device_id={"dp": lax.rem(y + dy, 4)}, device_id_type=MESH)
 
     def local(src, dst, i):
         cp = pltpu.make_async_copy(src, dst, loc_sem.at[i])
@@ -58,6 +61,8 @@
 
     cq = pl.ds(pl.multiple_of(x * 128, 128), 128)
     cv = pl.ds(pl.multiple_of(x * 256, 256), 256)
+    ld_tok = local(tokens, tok_in.at[x, c], 8)
+    ld_gains = [local(gain_mix_h, gain_mix, 9), local(gain_mlp_h, gain_mlp, 10)]
     ld_w = [
         local(w_query.at[:, cq], wbuf.at[x, :, 0:128], 0),
         local(w_key.at[:, cq], wbuf.at[x, :, 128:256], 1),
@@ -69,11 +74,8 @@
     ld_up = local(w_up, wup.at[c], 6)
     ld_dn = local(w_down, wdn.at[c], 7)
 
-    t32 = tokens[...].astype(F32)
-    packed = jnp.concatenate([t32[:128], t32[128:]], axis=1).astype(BF16)
-    tok_in[x, c] = packed
-
-    pl.semaphore_wait(bar, 35)
+    ld_tok.wait()
+    pl.semaphore_wait(bar, 38)
 
     def remote(src, dst, ss, rs, dev):
         cp = pltpu.make_async_remote_copy(
@@ -109,14 +111,9 @@
 
     for cp in tok_cp:
         cp.wait_recv()
-    low = lax.broadcasted_iota(jnp.int32, (128, 128), 1) < 64
     squares = jnp.zeros((256, 128), F32)
     for xx in range(NX):
-        a = tok_in[xx, 0].astype(F32)
-        b = tok_in[xx, 1].astype(F32)
-        top = jnp.where(low, a, pltpu.roll(b, 64, 1))
-        bottom = jnp.where(low, pltpu.roll(a, 64, 1), b)
-        both = jnp.concatenate([top, bottom], axis=0)
+        both = jnp.transpose(tok_in[xx].reshape(128, 256).astype(F32))
         tokf[:, :, xx * 128:(xx + 1) * 128] = both.reshape(32, 8, 128)
         squares = squares + both * both
     ssq_s[...] = jnp.broadcast_to(jnp.sum(squares, axis=1, keepdims=True), (256, 128)).reshape(32, 8, 128)
@@ -126,6 +123,8 @@
             remote(ssq_s.at[zp(dz) * NX + x], ssq_r.at[dz], ssq_ss.at[dz], ssq_rs.at[dz], {"kv_0": zp(dz)})
         )
     fz = pl.ds(pl.multiple_of(z * 512, 512), 512)
+    for ld in ld_gains:
+        ld.wait()
     normed = (tokf[...].reshape(256, 512) * gain_mix[:, fz]).astype(BF16)
 
     for ch in range(3):
@@ -146,9 +145,12 @@
 
         lax.fori_loop(1, NZ * NX, scatter, 0)
 
+    qrows = pl.ds(pl.multiple_of(y * 256, 256), 256)
     mix_cp = []
     for dx in (2, 1, 3):
-        mix_cp.append(remote(w_mix, wm.at[x], mix_ss.at[dx], mix_rs.at[dx], {"kv_1": xp(dx)}))
+        mix_cp.append(
+            remote(w_mix.at[qrows], wm.at[x, qrows], mix_ss.at[dx], mix_rs.at[dx], {"kv_1": xp(dx)})
+        )
 
     for cp in ssq_cp:
         cp.wait_recv()
@@ -164,47 +166,48 @@
         return (summed * scale16).astype(BF16).astype(F32)
 
     qk = own(0)
-    qs = qk[:, :8].reshape(32, 128)
-    ks = qk[:, 8:].reshape(32, 128) * 0.125
+    for dx in range(NX):
+        qk_abs[xp(NX - dx)] = qk[dx]
+    vals = own(1)
+    for dx in range(NX):
+        v_abs[xp(NX - dx)] = vals[dx]
+    my_cp = []
+    for i, dx in enumerate((2, 1, 3)):
+        mix_cp[i].wait_recv()
+        src = wm.at[xp(NX - dx), qrows]
+        for dy in (2, 1, 3):
+            my_cp.append(remote(src, src, my_ss.at[dx, dy], my_rs.at[dx, dy], {"dp": lax.rem(y + dy, 4)}))
+    qs = qk_abs[:, :8].reshape(32, 128)
+    ks = qk_abs[:, 8:].reshape(32, 128) * 0.125
     turned = jnp.transpose(jnp.concatenate([qs, ks, jnp.zeros((64, 128), F32)], axis=0))
-    vals = own(1)
+    keys_out[...] = turned
+    vals_out[...] = v_abs[...]
     ld_st.wait()
-    ns_cp = []
-    decays = []
-    for dx in range(NX):
-        xs = xp(NX - dx)
-        pair = []
-        for hh in range(2):
-            rate = rates[c * 8 + xs * 2 + hh]
-            pair.append(jnp.exp(-jnp.full((1, 128), rate, F32)))
-        decays.append(pair)
-    for b in range(8):
-        for dx in range(NX):
-            xs = xp(NX - dx)
+    decays = [jnp.exp(-jnp.full((1, 128), rates[c * 8 + h], F32)) for h in range(8)]
+    for xs in range(NX):
+        for b in range(8):
             for hh in range(2):
                 rows = slice(hh * 64, (hh + 1) * 64)
-                col = dx * 8 + b
-                old = st[b, xs, rows, :]
-                new = decays[dx][hh] * old + turned[rows, 32 + col:33 + col] * vals[dx, hh * 8 + b:hh * 8 + b + 1, :]
-                st[b, xs, rows, :] = new
-                rdbuf[dx, hh * 8 + b:hh * 8 + b + 1, :] = jnp.sum(
+                col = xs * 8 + b
+                new = decays[xs * 2 + hh] * st[b, xs, rows, :] + (
+                    turned[rows, 32 + col:33 + col] * v_abs[xs, hh * 8 + b:hh * 8 + b + 1, :]
+                )
+                rdbuf[xs, hh * 8 + b:hh * 8 + b + 1, :] = jnp.sum(
                     turned[rows, col:col + 1] * new, axis=0, keepdims=True
                 )
-        cp = pltpu.make_async_copy(st.at[b], new_state.at[b], ns_sem.at[b])
-        cp.start()
-        ns_cp.append(cp)
     gates = own(2)
+    for dx in range(NX):
+        g_abs[xp(NX - dx)] = gates[dx]
+    gates = g_abs[...]
     read = rdbuf[...]
     read = read * lax.rsqrt(jnp.mean(read * read, axis=2, keepdims=True) + EPS)
-    heads = (gates / (1.0 + jnp.exp(-gates)) * read).astype(BF16)
-    for dx in range(NX):
-        hall[z, xp(NX - dx)] = heads[dx]
+    hall[z] = (gates / (1.0 + jnp.exp(-gates)) * read).astype(BF16)
     h_cp = []
     for dz in FAR:
         h_cp.append(remote(hall.at[z], hall.at[z], h_ss.at[dz], h_rs.at[dz], {"kv_0": zp(dz)}))
     for cp in h_cp:
         cp.wait_recv()
-    for cp in mix_cp:
+    for cp in my_cp:
         cp.wait_recv()
     ld_mix.wait()
 
@@ -227,7 +230,7 @@
     rg[x, z] = (jnp.concatenate(own_tok, axis=0) + mixed).astype(BF16)
 
     rz_cp = {}
-    for dz in FAR:
+    for dz in (1, 7, 2, 6, 3, 5, 4):
         rz_cp[dz] = remote(rg.at[x, z], rg.at[x, z], rz_ss.at[dz], rz_rs.at[dz], {"kv_0": zp(dz)})
     rx_cp = []
     ORDER = (0, 1, 7, 2, 6, 3, 5, 4)
@@ -303,16 +306,38 @@
             for zl in range(4):
                 r0 = xs * 32 + zl * 8
                 fin[(who * 4 + zl) * NX + xs] = block[r0:r0 + 8]
-    done = fin[...].reshape(256, 128)
-    out[...] = jnp.where(c == 0, done, pltpu.roll(done, 64, 1))[:, :64].astype(BF16)
-
-    for cp in tok_cp + w_cp[0] + w_cp[1] + w_cp[2] + mlp_cp + ssq_cp + mix_cp + h_cp + [pr_cp]:
+    fint[...] = jnp.transpose(fin[...].reshape(256, 128))
+    out[...] = fint[pl.ds(pl.multiple_of(c * 64, 64), 64), :].astype(BF16)
+
+    for cp in tok_cp + w_cp[0] + w_cp[1] + w_cp[2] + mlp_cp + ssq_cp + mix_cp + my_cp + h_cp + [pr_cp]:
         cp.wait_send()
     for ch in range(3):
         pltpu.make_async_copy(sbuf.at[ch, 1:32], sbuf.at[ch, 1:32], p1_ss.at[ch]).wait()
     for cp in list(rz_cp.values()) + rx_cp + list(xs_cp.values()) + list(zs_cp.values()) + [f_cp]:
         cp.wait_send()
-    for cp in ns_cp:
+
+
+def tail(rates, keys, vals, res_in, state, result, new_state, st, ld_sem, out_sem):
+    c = lax.axis_index("tp")
+    loads = [pltpu.make_async_copy(state.at[b], st.at[b], ld_sem.at[b]) for b in range(8)]
+    for cp in loads:
+        cp.start()
+    result[...] = res_in[...]
+    decays = [jnp.exp(-jnp.full((1, 128), rates[c * 8 + h], F32)) for h in range(8)]
+    stores = []
+    for b in range(8):
+        loads[b].wait()
+        for xs in range(NX):
+            for hh in range(2):
+                rows = slice(hh * 64, (hh + 1) * 64)
+                col = 32 + xs * 8 + b
+                st[b, xs, rows, :] = decays[xs * 2 + hh] * st[b, xs, rows, :] + (
+                    keys[rows, col:col + 1] * vals[xs, hh * 8 + b:hh * 8 + b + 1, :]
+                )
+        cp = pltpu.make_async_copy(st.at[b], new_state.at[b], out_sem.at[b])
+        cp.start()
+        stores.append(cp)
+    for cp in stores:
         cp.wait()
 
 
@@ -320,19 +345,23 @@
     tokens, gain_mix, gain_mlp, decay_rate, w_query, w_key, w_value, w_gate, w_mix, w_up, w_down, state
 ):
     vm = pl.BlockSpec(memory_space=pltpu.VMEM)
+    sm = pl.BlockSpec(memory_space=pltpu.SMEM)
     hbm = pl.BlockSpec(memory_space=pltpu.HBM)
     dma = pltpu.SemaphoreType.DMA
-    result, new_state = pl.pallas_call(
+    state = state.reshape(8, 4, 128, 128)
+    result, keys, vals = pl.pallas_call(
         kernel,
         out_shape=(
-            jax.ShapeDtypeStruct((256, 64), BF16),
-            jax.ShapeDtypeStruct((8, 4, 128, 128), F32),
+            jax.ShapeDtypeStruct((64, 256), BF16),
+            jax.ShapeDtypeStruct((128, 128), F32),
+            jax.ShapeDtypeStruct((4, 16, 128), F32),
         ),
-        in_specs=[vm, vm, vm, pl.BlockSpec(memory_space=pltpu.SMEM)] + [hbm] * 8,
-        out_specs=(vm, hbm),
+        in_specs=[hbm, hbm, hbm, sm] + [hbm] * 8,
+        out_specs=(vm, vm, vm),
         scratch_shapes=[
-            pltpu.VMEM((128, 128), BF16),
-            pltpu.VMEM((4, 2, 128, 128), BF16),
+            pltpu.VMEM((1, 4096), F32),
+            pltpu.VMEM((1, 4096), F32),
+            pltpu.VMEM((4, 2, 64, 256), BF16),
             pltpu.VMEM((32, 8, 512), F32),
             pltpu.VMEM((4, 128, 768), BF16),
             pltpu.VMEM((4, 1024, 128), BF16),
@@ -343,6 +372,9 @@
             pltpu.VMEM((3, 32, 16, 128), BF16),
             pltpu.VMEM((32, 8, 128), F32),
             pltpu.VMEM((8, 8, 128), F32),
+            pltpu.VMEM((4, 16, 128), F32),
+            pltpu.VMEM((4, 16, 128), F32),
+            pltpu.VMEM((4, 16, 128), F32),
             pltpu.VMEM((4, 16, 128), F32),
             pltpu.VMEM((8, 4, 16, 128), BF16),
             pltpu.VMEM((2, 32, 512), BF16),
@@ -355,7 +387,8 @@
             pltpu.VMEM((128, 128), BF16),
             pltpu.VMEM((128, 128), BF16),
             pltpu.VMEM((32, 8, 128), F32),
-            dma((8,)), dma((8,)), dma((7,)), dma((7,)), dma((4, 4)), dma((4, 4)), dma((4,)), dma((4,)),
+            pltpu.VMEM((128, 256), F32),
+            dma((11,)), dma((7,)), dma((7,)), dma((4, 4)), dma((4, 4)), dma((4,)), dma((4,)), dma((4, 4)), dma((4, 4)),
             dma((2,)), dma((2,)), dma((3,)), dma((3,)), dma((8,)), dma((8,)), dma((8,)), dma((8,)),
             dma, dma, dma((8,)), dma((8,)), dma((8, 4)), dma((8, 4)), dma((8, 4)), dma((8, 4)),
             dma((8,)), dma((8,)), dma, dma,
@@ -365,10 +398,21 @@
         ),
         name="layer",
     )(
-        tokens, gain_mix.reshape(1, 4096), gain_mlp.reshape(1, 4096), decay_rate,
-        w_query, w_key, w_value, w_gate, w_mix, w_up, w_down, state.reshape(8, 4, 128, 128),
+        tokens.T, gain_mix.reshape(1, 4096), gain_mlp.reshape(1, 4096), decay_rate,
+        w_query, w_key, w_value, w_gate, w_mix, w_up, w_down, state,
     )
-    return result, new_state.reshape(8, 8, 64, 128)
+    result, new_state = pl.pallas_call(
+        tail,
+        out_shape=(
+            jax.ShapeDtypeStruct((64, 256), BF16),
+            jax.ShapeDtypeStruct((8, 4, 128, 128), F32),
+        ),
+        in_specs=[sm, vm, vm, vm, hbm],
+        out_specs=(vm, hbm),
+        scratch_shapes=[pltpu.VMEM((8, 4, 128, 128), F32), dma((8,)), dma((8,))],
+        name="tail",
+    )(decay_rate, keys, vals, result, state)
+    return result.T, new_state.reshape(8, 8, 64, 128)
 
 
 def solution(mesh):

time: 89.7 us -> 86.3 us (0.962)
  local copies, waits for them, and re-layouts: 6.19 us -> 0 us
  Pallas kernels: 82.6 us -> 85.5 us
    unnamed x3 -> x0, local copies, waits for them, and re-layouts: 6.19 us -> none
    pallas_call x1 -> x2, Pallas kernels: 82.6 us -> 85.5 us  [the longest x1 81.1 us: per_device(): pl.pallas_call(kernel, out_shape=(jax.ShapeDtypeStruct((64, 256), BF16),...]
where the time goes in v2:
time: 86.3 us; the launch traced here: 86.2 us
  Pallas kernels  85.5 us (99%)
    pallas_call x1, Pallas kernels, per_device(): pl.pallas_call(kernel, out_shape=(jax.ShapeDtypeStruct((64, 256), BF16),...  81.1 us
    pallas_call x1, Pallas kernels, per_device(): pl.pallas_call(tail, out_shape=(jax.ShapeDtypeStruct((64, 256), BF16), ja...  4.41 us

profile of v2, /device:TPU:1, one launch (start us, length us, event | category | flops | bytes accessed | tf_op | source)
XLA Modules:
  0.0 86.2 jit_solution(16484931348387020995)
XLA Ops:
  0.6 81.1 %layer.1 = (bf16[64,256]{1,0:T(8,128)(2,1)}, f32[128,128]{1,0:T(8,128)}, f32[4,16,128]{2,1,0:T(8,128)}) custom-call(bf16[64,256]{1,0:T(8,128)(2,1)} %bitcast.8, f32[1,4096]{1,0:T(1,128)} %bitcast.9, f32[1,4096]{1,0:T(1,128)} %bitcast.10, f32[16]{0:T(128)} %rates.3, bf16[128,512]{1,0:T(8,128)(2,1)} %w_query.1, bf16[128,512]{1,0:T(8,128)(2,1)} %w_key.1, ...), custom_call_target="tpu_custom_call" | custom-call | tf_op jit(solution)/shard_map/layer/pallas_call | solution.py:352
  81.8 4.4 %tail.1 = (bf16[64,256]{1,0:T(8,128)(2,1)}, f32[8,4,128,128]{3,2,1,0:T(8,128)}) custom-call(f32[16]{0:T(128)} %rates.3, f32[128,128]{1,0:T(8,128)} %get-tuple-element.7.keys, f32[4,16,128]{2,1,0:T(8,128)} %get-tuple-element.8.vals, bf16[64,256]{1,0:T(8,128)(2,1)} %get-tuple-element.9.res_in, f32[8,4,128,128]{3,2,1,0:T(8,128)} %bitcast.7), custom_call_target="tpu_custom_call" | custom-call | tf_op jit(solution)/shard_map/tail/pallas_call | solution.py:404

commit v3 on v2

--- a/solution.py
+++ b/solution.py
@@ -85,9 +85,11 @@
         return cp
 
     tok_cp = []
-    for i, (dx, other) in enumerate([(2, 0), (2, 1), (1, 0), (3, 0), (1, 1), (3, 1), (0, 1)]):
-        dev = {"kv_1": xp(dx), "tp": (1 - c) if other else c}
-        tok_cp.append(remote(tok_in.at[x, c], tok_in.at[x, c], tok_ss.at[i], tok_rs.at[i], dev))
+    for dx in (2, 1, 3):
+        tok_cp.append(
+            remote(tok_in.at[x, c], tok_in.at[x, c], tok_ss.at[dx], tok_rs.at[dx], {"kv_1": xp(dx)})
+        )
+    tokp_cp = [remote(tok_in.at[x, c], tok_in.at[x, c], tok_ss.at[4], tok_rs.at[4], {"tp": 1 - c})]
 
     w_cp = {0: [], 1: [], 2: []}
     for dx in (2, 1, 3):
@@ -103,13 +105,24 @@
                 remote(w.at[:, dv], wbuf.at[x, :, lo:lo + 256], w_ss.at[2 + j, dx], w_rs.at[2 + j, dx], dev)
             )
 
+    qrows = pl.ds(pl.multiple_of(y * 256, 256), 256)
+    mix_cp = []
+    for dx in (2, 1, 3):
+        mix_cp.append(
+            remote(w_mix.at[qrows], wm.at[x, qrows], mix_ss.at[dx], mix_rs.at[dx], {"kv_1": xp(dx)})
+        )
+
     partner = {"tp": 1 - c}
     mlp_cp = [
         remote(w_up, wup.at[c], mlp_ss.at[0], mlp_rs.at[0], partner),
         remote(w_down, wdn.at[c], mlp_ss.at[1], mlp_rs.at[1], partner),
     ]
 
-    for cp in tok_cp:
+    for i, dx in enumerate((1, 3, 2)):
+        tok_cp[(1, 2, 0)[i]].wait_recv()
+        src = tok_in.at[xp(NX - dx), c]
+        tokp_cp.append(remote(src, src, tok_ss.at[4 + dx], tok_rs.at[4 + dx], {"tp": 1 - c}))
+    for cp in tokp_cp:
         cp.wait_recv()
     squares = jnp.zeros((256, 128), F32)
     for xx in range(NX):
@@ -145,12 +158,12 @@
 
         lax.fori_loop(1, NZ * NX, scatter, 0)
 
-    qrows = pl.ds(pl.multiple_of(y * 256, 256), 256)
-    mix_cp = []
-    for dx in (2, 1, 3):
-        mix_cp.append(
-            remote(w_mix.at[qrows], wm.at[x, qrows], mix_ss.at[dx], mix_rs.at[dx], {"kv_1": xp(dx)})
-        )
+    my_cp = []
+    for i, dx in enumerate((2, 1, 3)):
+        mix_cp[i].wait_recv()
+        src = wm.at[xp(NX - dx), qrows]
+        for dy in (2, 1, 3):
+            my_cp.append(remote(src, src, my_ss.at[dx, dy], my_rs.at[dx, dy], {"dp": lax.rem(y + dy, 4)}))
 
     for cp in ssq_cp:
         cp.wait_recv()
@@ -171,12 +184,6 @@
     vals = own(1)
     for dx in range(NX):
         v_abs[xp(NX - dx)] = vals[dx]
-    my_cp = []
-    for i, dx in enumerate((2, 1, 3)):
-        mix_cp[i].wait_recv()
-        src = wm.at[xp(NX - dx), qrows]
-        for dy in (2, 1, 3):
-            my_cp.append(remote(src, src, my_ss.at[dx, dy], my_rs.at[dx, dy], {"dp": lax.rem(y + dy, 4)}))
     qs = qk_abs[:, :8].reshape(32, 128)
     ks = qk_abs[:, 8:].reshape(32, 128) * 0.125
     turned = jnp.transpose(jnp.concatenate([qs, ks, jnp.zeros((64, 128), F32)], axis=0))
@@ -309,7 +316,7 @@
     fint[...] = jnp.transpose(fin[...].reshape(256, 128))
     out[...] = fint[pl.ds(pl.multiple_of(c * 64, 64), 64), :].astype(BF16)
 
-    for cp in tok_cp + w_cp[0] + w_cp[1] + w_cp[2] + mlp_cp + ssq_cp + mix_cp + my_cp + h_cp + [pr_cp]:
+    for cp in tok_cp + tokp_cp + w_cp[0] + w_cp[1] + w_cp[2] + mlp_cp + ssq_cp + mix_cp + my_cp + h_cp + [pr_cp]:
         cp.wait_send()
     for ch in range(3):
         pltpu.make_async_copy(sbuf.at[ch, 1:32], sbuf.at[ch, 1:32], p1_ss.at[ch]).wait()
@@ -317,13 +324,20 @@
         cp.wait_send()
 
 
-def tail(rates, keys, vals, res_in, state, result, new_state, st, ld_sem, out_sem):
+def tail(rates, keys_h, vals_h, res_in, state, result, new_state, st, keys, vals, res, ld_sem, out_sem):
     c = lax.axis_index("tp")
-    loads = [pltpu.make_async_copy(state.at[b], st.at[b], ld_sem.at[b]) for b in range(8)]
-    for cp in loads:
+
+    def load(src, dst, i):
+        cp = pltpu.make_async_copy(src, dst, ld_sem.at[i])
         cp.start()
-    result[...] = res_in[...]
+        return cp
+
+    small = [load(keys_h, keys, 8), load(vals_h, vals, 9)]
+    loads = [load(state.at[b], st.at[b], b) for b in range(8)]
+    res_cp = load(res_in, res, 10)
     decays = [jnp.exp(-jnp.full((1, 128), rates[c * 8 + h], F32)) for h in range(8)]
+    for cp in small:
+        cp.wait()
     stores = []
     for b in range(8):
         loads[b].wait()
@@ -334,9 +348,12 @@
                 st[b, xs, rows, :] = decays[xs * 2 + hh] * st[b, xs, rows, :] + (
                     keys[rows, col:col + 1] * vals[xs, hh * 8 + b:hh * 8 + b + 1, :]
                 )
-        cp = pltpu.make_async_copy(st.at[b], new_state.at[b], out_sem.at[b])
-        cp.start()
-        stores.append(cp)
+        stores.append(pltpu.make_async_copy(st.at[b], new_state.at[b], out_sem.at[b]))
+        stores[-1].start()
+        if b == 0:
+            res_cp.wait()
+            stores.append(pltpu.make_async_copy(res, result, out_sem.at[8]))
+            stores[-1].start()
     for cp in stores:
         cp.wait()
 
@@ -388,7 +405,7 @@
             pltpu.VMEM((128, 128), BF16),
             pltpu.VMEM((32, 8, 128), F32),
             pltpu.VMEM((128, 256), F32),
-            dma((11,)), dma((7,)), dma((7,)), dma((4, 4)), dma((4, 4)), dma((4,)), dma((4,)), dma((4, 4)), dma((4, 4)),
+            dma((11,)), dma((8,)), dma((8,)), dma((4, 4)), dma((4, 4)), dma((4,)), dma((4,)), dma((4, 4)), dma((4, 4)),
             dma((2,)), dma((2,)), dma((3,)), dma((3,)), dma((8,)), dma((8,)), dma((8,)), dma((8,)),
             dma, dma, dma((8,)), dma((8,)), dma((8, 4)), dma((8, 4)), dma((8, 4)), dma((8, 4)),
             dma((8,)), dma((8,)), dma, dma,
@@ -407,9 +424,16 @@
             jax.ShapeDtypeStruct((64, 256), BF16),
             jax.ShapeDtypeStruct((8, 4, 128, 128), F32),
         ),
-        in_specs=[sm, vm, vm, vm, hbm],
-        out_specs=(vm, hbm),
-        scratch_shapes=[pltpu.VMEM((8, 4, 128, 128), F32), dma((8,)), dma((8,))],
+        in_specs=[sm, hbm, hbm, hbm, hbm],
+        out_specs=(hbm, hbm),
+        scratch_shapes=[
+            pltpu.VMEM((8, 4, 128, 128), F32),
+            pltpu.VMEM((128, 128), F32),
+            pltpu.VMEM((4, 16, 128), F32),
+            pltpu.VMEM((64, 256), BF16),
+            dma((11,)), dma((9,)),
+        ],
+        compiler_params=pltpu.CompilerParams(vmem_limit_bytes=60 * 1024 * 1024),
         name="tail",
     )(decay_rate, keys, vals, result, state)
     return result.T, new_state.reshape(8, 8, 64, 128)

time: 86.3 us -> 80.9 us (0.937)
  Pallas kernels: 85.5 us -> 80.1 us
    pallas_call x1, Pallas kernels: 81.1 us -> 76.1 us  [per_device(): pl.pallas_call(kernel, out_shape=(jax.ShapeDtypeStruct((64, 256), BF16),...]
where the time goes in v3:
time: 80.9 us; the launch traced here: 80.8 us
  Pallas kernels  80.1 us (99%)
    pallas_call x1, Pallas kernels, per_device(): pl.pallas_call(kernel, out_shape=(jax.ShapeDtypeStruct((64, 256), BF16),...  76.1 us
    pallas_call x1, Pallas kernels, per_device(): pl.pallas_call(tail, out_shape=(jax.ShapeDtypeStruct((64, 256), BF16), ja...  3.97 us

profile of v3, /device:TPU:1, one launch (start us, length us, event | category | flops | bytes accessed | tf_op | source)
XLA Modules:
  0.0 80.8 jit_solution(11636244747775426219)
XLA Ops:
  0.6 76.1 %layer.1 = (bf16[64,256]{1,0:T(8,128)(2,1)}, f32[128,128]{1,0:T(8,128)}, f32[4,16,128]{2,1,0:T(8,128)}) custom-call(bf16[64,256]{1,0:T(8,128)(2,1)} %bitcast.8, f32[1,4096]{1,0:T(1,128)} %bitcast.9, f32[1,4096]{1,0:T(1,128)} %bitcast.10, f32[16]{0:T(128)} %rates.3, bf16[128,512]{1,0:T(8,128)(2,1)} %w_query.1, bf16[128,512]{1,0:T(8,128)(2,1)} %w_key.1, ...), custom_call_target="tpu_custom_call" | custom-call | tf_op jit(solution)/shard_map/layer/pallas_call | solution.py:369
  76.8 4.0 %tail.1 = (bf16[64,256]{1,0:T(8,128)(2,1)}, f32[8,4,128,128]{3,2,1,0:T(8,128)}) custom-call(f32[16]{0:T(128)} %rates.3, f32[128,128]{1,0:T(8,128)} %get-tuple-element.7.keys_h, f32[4,16,128]{2,1,0:T(8,128)} %get-tuple-element.8.vals_h, bf16[64,256]{1,0:T(8,128)(2,1)} %get-tuple-element.9.res_in, f32[8,4,128,128]{3,2,1,0:T(8,128)} %bitcast.7), custom_call_target="tpu_custom_call" | custom-call | tf_op jit(solution)/shard_map/tail/pallas_call | solution.py:421

commit v4 on v3

--- a/solution.py
+++ b/solution.py
@@ -23,10 +23,10 @@
     out, keys_out, vals_out,
     gain_mix, gain_mlp, tok_in, tokf, wbuf, wm, wup, wdn, st,
     sbuf, rbuf, ssq_s, ssq_r, qk_abs, v_abs, g_abs, rdbuf, hall, pbuf, pin, rg,
-    xsb, xrb, zsb, zrb, fsend, frecv, fin, fint,
+    xsb, xrb, zsb, zrb, bzs, bzr, bxs, bxr, fsend, frecv, fin, fint,
     loc_sem, tok_ss, tok_rs, w_ss, w_rs, mix_ss, mix_rs, my_ss, my_rs, mlp_ss, mlp_rs,
     p1_ss, p1_rs, ssq_ss, ssq_rs, h_ss, h_rs, pr_ss, pr_rs,
-    rz_ss, rz_rs, rx_ss, rx_rs, xs_ss, xs_rs, zs_ss, zs_rs, f_ss, f_rs,
+    rz_ss, rz_rs, rx_ss, rx_rs, xs_ss, xs_rs, zs_ss, zs_rs, bz_ss, bz_rs, bx_ss, bx_rs, f_ss, f_rs,
 ):
     z = lax.axis_index("kv_0")
     x = lax.axis_index("kv_1")
@@ -274,6 +274,7 @@
     ld_dn.wait()
     mlp_cp[1].wait_recv()
     xs_cp = {}
+    bz_cp = {}
     for i in range(NZ):
         dz = (FAR + (0,))[i]
         zz = zp(dz)
@@ -282,7 +283,10 @@
         part = part + jnp.dot(hid[1], wdn[1, :, fk], preferred_element_type=F32)
         part = part.astype(BF16)
         for xx in range(NX):
-            xsb[dz, xx] = part[:, xx * 128:(xx + 1) * 128]
+            xsb[dz, xx] = part[:96, xx * 128:(xx + 1) * 128]
+            bzs[dz, xx] = part[96:, xx * 128:(xx + 1) * 128]
+        if dz:
+            bz_cp[dz] = remote(bzs.at[dz], bzr.at[dz - 1], bz_ss.at[dz], bz_rs.at[dz], {"kv_0": zp(dz)})
         for dx in (2, 1, 3):
             xs_cp[dz, dx] = remote(
                 xsb.at[dz, xp(dx)], xrb.at[dz, dx - 1], xs_ss.at[dz, dx], xs_rs.at[dz, dx], {"kv_1": xp(dx)}
@@ -300,8 +304,21 @@
         else:
             own_sum = summed
     for dz in FAR:
+        bz_cp[dz].wait_recv()
+    last = bzs[0].astype(F32) + jnp.sum(bzr[...].astype(F32), axis=0)
+    bxs[...] = last.astype(BF16)
+    bx_cp = []
+    for dx in (2, 1, 3):
+        bx_cp.append(
+            remote(bxs.at[xp(dx)], bxr.at[dx - 1], bx_ss.at[dx], bx_rs.at[dx], {"kv_1": xp(dx)})
+        )
+    for dz in FAR:
         zs_cp[dz].wait_recv()
-    down = own_sum + jnp.sum(zrb[...].astype(F32), axis=0)
+    first = own_sum + jnp.sum(zrb[...].astype(F32), axis=0)
+    for cp in bx_cp:
+        cp.wait_recv()
+    last = bxs[x].astype(F32) + jnp.sum(bxr[...].astype(F32), axis=0)
+    down = jnp.concatenate([first, last], axis=0)
     lanes = pl.ds(pl.multiple_of(x * 128, 128), 128)
     res = rg[:, z, :, lanes].reshape(128, 128).astype(F32)
     fsend[...] = (res + down).astype(BF16)
@@ -320,7 +337,7 @@
         cp.wait_send()
     for ch in range(3):
         pltpu.make_async_copy(sbuf.at[ch, 1:32], sbuf.at[ch, 1:32], p1_ss.at[ch]).wait()
-    for cp in list(rz_cp.values()) + rx_cp + list(xs_cp.values()) + list(zs_cp.values()) + [f_cp]:
+    for cp in list(rz_cp.values()) + rx_cp + list(xs_cp.values()) + list(zs_cp.values()) + list(bz_cp.values()) + bx_cp + [f_cp]:
         cp.wait_send()
 
 
@@ -397,10 +414,14 @@
             pltpu.VMEM((2, 32, 512), BF16),
             pltpu.VMEM((32, 512), BF16),
             pltpu.VMEM((4, 8, 32, 512), BF16),
-            pltpu.VMEM((8, 4, 128, 128), BF16),
-            pltpu.VMEM((8, 3, 128, 128), BF16),
-            pltpu.VMEM((8, 128, 128), BF16),
-            pltpu.VMEM((7, 128, 128), BF16),
+            pltpu.VMEM((8, 4, 96, 128), BF16),
+            pltpu.VMEM((8, 3, 96, 128), BF16),
+            pltpu.VMEM((8, 96, 128), BF16),
+            pltpu.VMEM((7, 96, 128), BF16),
+            pltpu.VMEM((8, 4, 32, 128), BF16),
+            pltpu.VMEM((7, 4, 32, 128), BF16),
+            pltpu.VMEM((4, 32, 128), BF16),
+            pltpu.VMEM((3, 32, 128), BF16),
             pltpu.VMEM((128, 128), BF16),
             pltpu.VMEM((128, 128), BF16),
             pltpu.VMEM((32, 8, 128), F32),
@@ -408,7 +429,7 @@
             dma((11,)), dma((8,)), dma((8,)), dma((4, 4)), dma((4, 4)), dma((4,)), dma((4,)), dma((4, 4)), dma((4, 4)),
             dma((2,)), dma((2,)), dma((3,)), dma((3,)), dma((8,)), dma((8,)), dma((8,)), dma((8,)),
             dma, dma, dma((8,)), dma((8,)), dma((8, 4)), dma((8, 4)), dma((8, 4)), dma((8, 4)),
-            dma((8,)), dma((8,)), dma, dma,
+            dma((8,)), dma((8,)), dma((8,)), dma((8,)), dma((4,)), dma((4,)), dma, dma,
         ],
         compiler_params=pltpu.CompilerParams(
             collective_id=0, has_side_effects=True, vmem_limit_bytes=60 * 1024 * 1024

time: 80.9 us -> 78.7 us (0.973)
  Pallas kernels: 80.1 us -> 77.9 us
    pallas_call x1, Pallas kernels: 76.1 us -> 73.9 us  [per_device(): pl.pallas_call(kernel, out_shape=(jax.ShapeDtypeStruct((64, 256), BF16),...]
where the time goes in v4:
time: 78.7 us; the launch traced here: 78.5 us
  Pallas kernels  77.9 us (99%)
    pallas_call x1, Pallas kernels, per_device(): pl.pallas_call(kernel, out_shape=(jax.ShapeDtypeStruct((64, 256), BF16),...  73.9 us
    pallas_call x1, Pallas kernels, per_device(): pl.pallas_call(tail, out_shape=(jax.ShapeDtypeStruct((64, 256), BF16), ja...  3.97 us

profile of v4, /device:TPU:1, one launch (start us, length us, event | category | flops | bytes accessed | tf_op | source)
XLA Modules:
  0.0 78.5 jit_solution(2521297191941910971)
XLA Ops:
  0.6 73.9 %layer.1 = (bf16[64,256]{1,0:T(8,128)(2,1)}, f32[128,128]{1,0:T(8,128)}, f32[4,16,128]{2,1,0:T(8,128)}) custom-call(bf16[64,256]{1,0:T(8,128)(2,1)} %bitcast.8, f32[1,4096]{1,0:T(1,128)} %bitcast.9, f32[1,4096]{1,0:T(1,128)} %bitcast.10, f32[16]{0:T(128)} %rates.3, bf16[128,512]{1,0:T(8,128)(2,1)} %w_query.1, bf16[128,512]{1,0:T(8,128)(2,1)} %w_key.1, ...), custom_call_target="tpu_custom_call" | custom-call | tf_op jit(solution)/shard_map/layer/pallas_call | solution.py:386
  74.6 4.0 %tail.1 = (bf16[64,256]{1,0:T(8,128)(2,1)}, f32[8,4,128,128]{3,2,1,0:T(8,128)}) custom-call(f32[16]{0:T(128)} %rates.3, f32[128,128]{1,0:T(8,128)} %get-tuple-element.7.keys_h, f32[4,16,128]{2,1,0:T(8,128)} %get-tuple-element.8.vals_h, bf16[64,256]{1,0:T(8,128)(2,1)} %get-tuple-element.9.res_in, f32[8,4,128,128]{3,2,1,0:T(8,128)} %bitcast.7), custom_call_target="tpu_custom_call" | custom-call | tf_op jit(solution)/shard_map/tail/pallas_call | solution.py:442

commit v5 on v4

--- a/solution.py
+++ b/solution.py
@@ -20,11 +20,11 @@
 
 def kernel(
     tokens, gain_mix_h, gain_mlp_h, rates, w_query, w_key, w_value, w_gate, w_mix, w_up, w_down, state,
-    out, keys_out, vals_out,
+    out, new_state,
     gain_mix, gain_mlp, tok_in, tokf, wbuf, wm, wup, wdn, st,
     sbuf, rbuf, ssq_s, ssq_r, qk_abs, v_abs, g_abs, rdbuf, hall, pbuf, pin, rg,
     xsb, xrb, zsb, zrb, bzs, bzr, bxs, bxr, fsend, frecv, fin, fint,
-    loc_sem, tok_ss, tok_rs, w_ss, w_rs, mix_ss, mix_rs, my_ss, my_rs, mlp_ss, mlp_rs,
+    loc_sem, ns_sem, tok_ss, tok_rs, w_ss, w_rs, mix_ss, mix_rs, my_ss, my_rs, mlp_ss, mlp_rs,
     p1_ss, p1_rs, ssq_ss, ssq_rs, h_ss, h_rs, pr_ss, pr_rs,
     rz_ss, rz_rs, rx_ss, rx_rs, xs_ss, xs_rs, zs_ss, zs_rs, bz_ss, bz_rs, bx_ss, bx_rs, f_ss, f_rs,
 ):
@@ -49,8 +49,7 @@
         return 0
 
     lax.fori_loop(1, NZ * NX, greet, 0)
-    for dx in range(NX):
-        pl.semaphore_signal(bar, inc=1, device_id={"kv_1": xp(dx), "tp": 1 - c}, device_id_type=MESH)
+    pl.semaphore_signal(bar, inc=1, device_id={"tp": 1 - c}, device_id_type=MESH)
     for dy in range(1, 4):
         pl.semaphore_signal(bar, inc=1, device_id={"dp": lax.rem(y + dy, 4)}, device_id_type=MESH)
 
@@ -75,7 +74,7 @@
     ld_dn = local(w_down, wdn.at[c], 7)
 
     ld_tok.wait()
-    pl.semaphore_wait(bar, 38)
+    pl.semaphore_wait(bar, 35)
 
     def remote(src, dst, ss, rs, dev):
         cp = pltpu.make_async_remote_copy(
@@ -187,8 +186,6 @@
     qs = qk_abs[:, :8].reshape(32, 128)
     ks = qk_abs[:, 8:].reshape(32, 128) * 0.125
     turned = jnp.transpose(jnp.concatenate([qs, ks, jnp.zeros((64, 128), F32)], axis=0))
-    keys_out[...] = turned
-    vals_out[...] = v_abs[...]
     ld_st.wait()
     decays = [jnp.exp(-jnp.full((1, 128), rates[c * 8 + h], F32)) for h in range(8)]
     for xs in range(NX):
@@ -199,9 +196,15 @@
                 new = decays[xs * 2 + hh] * st[b, xs, rows, :] + (
                     turned[rows, 32 + col:33 + col] * v_abs[xs, hh * 8 + b:hh * 8 + b + 1, :]
                 )
+                st[b, xs, rows, :] = new
                 rdbuf[xs, hh * 8 + b:hh * 8 + b + 1, :] = jnp.sum(
                     turned[rows, col:col + 1] * new, axis=0, keepdims=True
                 )
+    ns_cp = []
+    for q in range(4):
+        cp = pltpu.make_async_copy(st.at[2 * q:2 * q + 2], new_state.at[2 * q:2 * q + 2], ns_sem.at[q])
+        cp.start()
+        ns_cp.append(cp)
     gates = own(2)
     for dx in range(NX):
         g_abs[xp(NX - dx)] = gates[dx]
@@ -339,38 +342,19 @@
         pltpu.make_async_copy(sbuf.at[ch, 1:32], sbuf.at[ch, 1:32], p1_ss.at[ch]).wait()
     for cp in list(rz_cp.values()) + rx_cp + list(xs_cp.values()) + list(zs_cp.values()) + list(bz_cp.values()) + bx_cp + [f_cp]:
         cp.wait_send()
-
-
-def tail(rates, keys_h, vals_h, res_in, state, result, new_state, st, keys, vals, res, ld_sem, out_sem):
-    c = lax.axis_index("tp")
-
-    def load(src, dst, i):
-        cp = pltpu.make_async_copy(src, dst, ld_sem.at[i])
+    for cp in ns_cp:
+        cp.wait()
+
+
+def tail(res_in, state_in, result, new_state, st, res, ld_sem, out_sem):
+    moves = [(state_in.at[b], st.at[b], new_state.at[b]) for b in range(8)] + [(res_in, res, result)]
+    loads = [pltpu.make_async_copy(src, held, ld_sem.at[i]) for i, (src, held, _) in enumerate(moves)]
+    stores = [pltpu.make_async_copy(held, dst, out_sem.at[i]) for i, (_, held, dst) in enumerate(moves)]
+    for cp in loads:
         cp.start()
-        return cp
-
-    small = [load(keys_h, keys, 8), load(vals_h, vals, 9)]
-    loads = [load(state.at[b], st.at[b], b) for b in range(8)]
-    res_cp = load(res_in, res, 10)
-    decays = [jnp.exp(-jnp.full((1, 128), rates[c * 8 + h], F32)) for h in range(8)]
-    for cp in small:
-        cp.wait()
-    stores = []
-    for b in range(8):
-        loads[b].wait()
-        for xs in range(NX):
-            for hh in range(2):
-                rows = slice(hh * 64, (hh + 1) * 64)
-                col = 32 + xs * 8 + b
-                st[b, xs, rows, :] = decays[xs * 2 + hh] * st[b, xs, rows, :] + (
-                    keys[rows, col:col + 1] * vals[xs, hh * 8 + b:hh * 8 + b + 1, :]
-                )
-        stores.append(pltpu.make_async_copy(st.at[b], new_state.at[b], out_sem.at[b]))
-        stores[-1].start()
-        if b == 0:
-            res_cp.wait()
-            stores.append(pltpu.make_async_copy(res, result, out_sem.at[8]))
-            stores[-1].start()
+    for i in range(9):
+        loads[i].wait()
+        stores[i].start()
     for cp in stores:
         cp.wait()
 
@@ -383,15 +367,14 @@
     hbm = pl.BlockSpec(memory_space=pltpu.HBM)
     dma = pltpu.SemaphoreType.DMA
     state = state.reshape(8, 4, 128, 128)
-    result, keys, vals = pl.pallas_call(
+    result, new_state = pl.pallas_call(
         kernel,
         out_shape=(
             jax.ShapeDtypeStruct((64, 256), BF16),
-            jax.ShapeDtypeStruct((128, 128), F32),
-            jax.ShapeDtypeStruct((4, 16, 128), F32),
+            jax.ShapeDtypeStruct((8, 4, 128, 128), F32),
         ),
         in_specs=[hbm, hbm, hbm, sm] + [hbm] * 8,
-        out_specs=(vm, vm, vm),
+        out_specs=(vm, hbm),
         scratch_shapes=[
             pltpu.VMEM((1, 4096), F32),
             pltpu.VMEM((1, 4096), F32),
@@ -426,7 +409,7 @@
             pltpu.VMEM((128, 128), BF16),
             pltpu.VMEM((32, 8, 128), F32),
             pltpu.VMEM((128, 256), F32),
-            dma((11,)), dma((8,)), dma((8,)), dma((4, 4)), dma((4, 4)), dma((4,)), dma((4,)), dma((4, 4)), dma((4, 4)),
+            dma((11,)), dma((4,)), dma((8,)), dma((8,)), dma((4, 4)), dma((4, 4)), dma((4,)), dma((4,)), dma((4, 4)), dma((4, 4)),
             dma((2,)), dma((2,)), dma((3,)), dma((3,)), dma((8,)), dma((8,)), dma((8,)), dma((8,)),
             dma, dma, dma((8,)), dma((8,)), dma((8, 4)), dma((8, 4)), dma((8, 4)), dma((8, 4)),
             dma((8,)), dma((8,)), dma((8,)), dma((8,)), dma((4,)), dma((4,)), dma, dma,
@@ -445,18 +428,16 @@
             jax.ShapeDtypeStruct((64, 256), BF16),
             jax.ShapeDtypeStruct((8, 4, 128, 128), F32),
         ),
-        in_specs=[sm, hbm, hbm, hbm, hbm],
+        in_specs=[hbm, hbm],
         out_specs=(hbm, hbm),
         scratch_shapes=[
             pltpu.VMEM((8, 4, 128, 128), F32),
-            pltpu.VMEM((128, 128), F32),
-            pltpu.VMEM((4, 16, 128), F32),
             pltpu.VMEM((64, 256), BF16),
-            dma((11,)), dma((9,)),
+            dma((9,)), dma((9,)),
         ],
         compiler_params=pltpu.CompilerParams(vmem_limit_bytes=60 * 1024 * 1024),
         name="tail",
-    )(decay_rate, keys, vals, result, state)
+    )(result, new_state)
     return result.T, new_state.reshape(8, 8, 64, 128)
 
 

time: 78.7 us -> 77.1 us (0.980)
  Pallas kernels: 77.9 us -> 76.4 us
    pallas_call x1, Pallas kernels: 3.97 us -> 2.41 us  [per_device(): pl.pallas_call(tail, out_shape=(jax.ShapeDtypeStruct((64, 256), BF16), ja...]
where the time goes in v5:
time: 77.1 us; the launch traced here: 77 us
  Pallas kernels  76.4 us (99%)
    pallas_call x1, Pallas kernels, per_device(): pl.pallas_call(kernel, out_shape=(jax.ShapeDtypeStruct((64, 256), BF16),...  74 us
    pallas_call x1, Pallas kernels, per_device(): pl.pallas_call(tail, out_shape=(jax.ShapeDtypeStruct((64, 256), BF16), ja...  2.41 us

profile of v5, /device:TPU:1, one launch (start us, length us, event | category | flops | bytes accessed | tf_op | source)
XLA Modules:
  0.0 77.0 jit_solution(16578341934852876168)
XLA Ops:
  0.6 74.0 %layer.1 = (bf16[64,256]{1,0:T(8,128)(2,1)}, f32[8,4,128,128]{3,2,1,0:T(8,128)}) custom-call(bf16[64,256]{1,0:T(8,128)(2,1)} %bitcast.7, f32[1,4096]{1,0:T(1,128)} %bitcast.8, f32[1,4096]{1,0:T(1,128)} %bitcast.9, f32[16]{0:T(128)} %rates.1, bf16[128,512]{1,0:T(8,128)(2,1)} %w_query.1, bf16[128,512]{1,0:T(8,128)(2,1)} %w_key.1, bf16[128,1024]{1,0:T(8,128)(2,1)} %w_value.1, ...), custom_call_target="tpu_custom_call" | custom-call | tf_op jit(solution)/shard_map/layer/pallas_call | solution.py:370
  74.6 2.4 %tail.1 = (bf16[64,256]{1,0:T(8,128)(2,1)}, f32[8,4,128,128]{3,2,1,0:T(8,128)}) custom-call(bf16[64,256]{1,0:T(8,128)(2,1)} %get-tuple-element.6.res_in, f32[8,4,128,128]{3,2,1,0:T(8,128)} %get-tuple-element.7.state_in), custom_call_target="tpu_custom_call" | custom-call | tf_op jit(solution)/shard_map/tail/pallas_call | solution.py:425

commit v6 on v5

--- a/solution.py
+++ b/solution.py
@@ -19,12 +19,12 @@
 
 
 def kernel(
-    tokens, gain_mix_h, gain_mlp_h, rates, w_query, w_key, w_value, w_gate, w_mix, w_up, w_down, state,
+    tokens, gain_mix_h, gain_mlp_h, rates_h, w_query, w_key, w_value, w_gate, w_mix, w_up, w_down, state,
     out, new_state,
     gain_mix, gain_mlp, tok_in, tokf, wbuf, wm, wup, wdn, st,
     sbuf, rbuf, ssq_s, ssq_r, qk_abs, v_abs, g_abs, rdbuf, hall, pbuf, pin, rg,
     xsb, xrb, zsb, zrb, bzs, bzr, bxs, bxr, fsend, frecv, fin, fint,
-    loc_sem, ns_sem, tok_ss, tok_rs, w_ss, w_rs, mix_ss, mix_rs, my_ss, my_rs, mlp_ss, mlp_rs,
+    rates, hop, loc_sem, ns_sem, tok_ss, tok_rs, w_ss, w_rs, mix_ss, mix_rs, my_ss, my_rs, mlp_ss, mlp_rs,
     p1_ss, p1_rs, ssq_ss, ssq_rs, h_ss, h_rs, pr_ss, pr_rs,
     rz_ss, rz_rs, rx_ss, rx_rs, xs_ss, xs_rs, zs_ss, zs_rs, bz_ss, bz_rs, bx_ss, bx_rs, f_ss, f_rs,
 ):
@@ -41,17 +41,11 @@
         return lax.rem(x + d, NX)
 
     bar = pltpu.get_barrier_semaphore()
-
-    def greet(i, _):
-        pl.semaphore_signal(
-            bar, inc=1, device_id={"kv_0": zp(i // NX), "kv_1": xp(i % NX)}, device_id_type=MESH
-        )
-        return 0
-
-    lax.fori_loop(1, NZ * NX, greet, 0)
-    pl.semaphore_signal(bar, inc=1, device_id={"tp": 1 - c}, device_id_type=MESH)
-    for dy in range(1, 4):
-        pl.semaphore_signal(bar, inc=1, device_id={"dp": lax.rem(y + dy, 4)}, device_id_type=MESH)
+    nearby = [{"tp": 1 - c}, {"kv_0": zp(1)}, {"kv_0": zp(NZ - 1)}]
+    nearby += [{"kv_1": xp(dx)} for dx in range(1, NX)]
+    nearby += [{"dp": lax.rem(y + dy, 4)} for dy in range(1, 4)]
+    for dev in nearby:
+        pl.semaphore_signal(bar, inc=1, device_id=dev, device_id_type=MESH)
 
     def local(src, dst, i):
         cp = pltpu.make_async_copy(src, dst, loc_sem.at[i])
@@ -61,7 +55,7 @@
     cq = pl.ds(pl.multiple_of(x * 128, 128), 128)
     cv = pl.ds(pl.multiple_of(x * 256, 256), 256)
     ld_tok = local(tokens, tok_in.at[x, c], 8)
-    ld_gains = [local(gain_mix_h, gain_mix, 9), local(gain_mlp_h, gain_mlp, 10)]
+    ld_gains = [local(gain_mix_h, gain_mix, 9), local(gain_mlp_h, gain_mlp, 10), local(rates_h, rates, 11)]
     ld_w = [
         local(w_query.at[:, cq], wbuf.at[x, :, 0:128], 0),
         local(w_key.at[:, cq], wbuf.at[x, :, 128:256], 1),
@@ -74,7 +68,9 @@
     ld_dn = local(w_down, wdn.at[c], 7)
 
     ld_tok.wait()
-    pl.semaphore_wait(bar, 35)
+    pl.semaphore_wait(bar, len(nearby))
+
+    partner = {"tp": 1 - c}
 
     def remote(src, dst, ss, rs, dev):
         cp = pltpu.make_async_remote_copy(
@@ -111,11 +107,11 @@
             remote(w_mix.at[qrows], wm.at[x, qrows], mix_ss.at[dx], mix_rs.at[dx], {"kv_1": xp(dx)})
         )
 
-    partner = {"tp": 1 - c}
-    mlp_cp = [
-        remote(w_up, wup.at[c], mlp_ss.at[0], mlp_rs.at[0], partner),
-        remote(w_down, wdn.at[c], mlp_ss.at[1], mlp_rs.at[1], partner),
-    ]
+    for r in range(4):
+        pl.semaphore_signal(hop.at[r, 0], inc=1, device_id={"kv_0": zp(1)}, device_id_type=MESH)
+        pl.semaphore_signal(hop.at[r, 1], inc=1, device_id={"kv_0": zp(NZ - 1)}, device_id_type=MESH)
+        pl.semaphore_wait(hop.at[r, 0], 1)
+        pl.semaphore_wait(hop.at[r, 1], 1)
 
     for i, dx in enumerate((1, 3, 2)):
         tok_cp[(1, 2, 0)[i]].wait_recv()
@@ -156,6 +152,11 @@
             return 0
 
         lax.fori_loop(1, NZ * NX, scatter, 0)
+
+    mlp_cp = [
+        remote(w_up, wup.at[c], mlp_ss.at[0], mlp_rs.at[0], partner),
+        remote(w_down, wdn.at[c], mlp_ss.at[1], mlp_rs.at[1], partner),
+    ]
 
     my_cp = []
     for i, dx in enumerate((2, 1, 3)):
@@ -363,7 +364,6 @@
     tokens, gain_mix, gain_mlp, decay_rate, w_query, w_key, w_value, w_gate, w_mix, w_up, w_down, state
 ):
     vm = pl.BlockSpec(memory_space=pltpu.VMEM)
-    sm = pl.BlockSpec(memory_space=pltpu.SMEM)
     hbm = pl.BlockSpec(memory_space=pltpu.HBM)
     dma = pltpu.SemaphoreType.DMA
     state = state.reshape(8, 4, 128, 128)
@@ -373,7 +373,7 @@
             jax.ShapeDtypeStruct((64, 256), BF16),
             jax.ShapeDtypeStruct((8, 4, 128, 128), F32),
         ),
-        in_specs=[hbm, hbm, hbm, sm] + [hbm] * 8,
+        in_specs=[hbm] * 12,
         out_specs=(vm, hbm),
         scratch_shapes=[
             pltpu.VMEM((1, 4096), F32),
@@ -409,7 +409,7 @@
             pltpu.VMEM((128, 128), BF16),
             pltpu.VMEM((32, 8, 128), F32),
             pltpu.VMEM((128, 256), F32),
-            dma((11,)), dma((4,)), dma((8,)), dma((8,)), dma((4, 4)), dma((4, 4)), dma((4,)), dma((4,)), dma((4, 4)), dma((4, 4)),
+            pltpu.SMEM((16,), F32), pltpu.SemaphoreType.REGULAR((4, 2)), dma((12,)), dma((4,)), dma((8,)), dma((8,)), dma((4, 4)), dma((4, 4)), dma((4,)), dma((4,)), dma((4, 4)), dma((4, 4)),
             dma((2,)), dma((2,)), dma((3,)), dma((3,)), dma((8,)), dma((8,)), dma((8,)), dma((8,)),
             dma, dma, dma((8,)), dma((8,)), dma((8, 4)), dma((8, 4)), dma((8, 4)), dma((8, 4)),
             dma((8,)), dma((8,)), dma((8,)), dma((8,)), dma((4,)), dma((4,)), dma, dma,

time: 77.1 us -> 75.6 us (0.981)
  Pallas kernels: 76.4 us -> 74.9 us
    pallas_call x1, Pallas kernels: 74 us -> 72.4 us  [per_device(): pl.pallas_call(kernel, out_shape=(jax.ShapeDtypeStruct((64, 256), BF16),...]
where the time goes in v6:
time: 75.6 us; the launch traced here: 75.5 us
  Pallas kernels  74.9 us (99%)
    pallas_call x1, Pallas kernels, per_device(): pl.pallas_call(kernel, out_shape=(jax.ShapeDtypeStruct((64, 256), BF16),...  72.4 us
    pallas_call x1, Pallas kernels, per_device(): pl.pallas_call(tail, out_shape=(jax.ShapeDtypeStruct((64, 256), BF16), ja...  2.41 us

profile of v6, /device:TPU:1, one launch (start us, length us, event | category | flops | bytes accessed | tf_op | source)
XLA Modules:
  0.0 75.5 jit_solution(18420984187579894014)
XLA Ops:
  0.6 72.4 %layer.1 = (bf16[64,256]{1,0:T(8,128)(2,1)}, f32[8,4,128,128]{3,2,1,0:T(8,128)}) custom-call(bf16[64,256]{1,0:T(8,128)(2,1)} %bitcast.7, f32[1,4096]{1,0:T(1,128)} %bitcast.8, f32[1,4096]{1,0:T(1,128)} %bitcast.9, f32[16]{0:T(128)} %rates_h.1, bf16[128,512]{1,0:T(8,128)(2,1)} %w_query.1, bf16[128,512]{1,0:T(8,128)(2,1)} %w_key.1, bf16[128,1024]{1,0:T(8,128)(2,1)} %w_value.1, ...), custom_call_target="tpu_custom_call" | custom-call | tf_op jit(solution)/shard_map/layer/pallas_call | solution.py:370
  73.1 2.4 %tail.1 = (bf16[64,256]{1,0:T(8,128)(2,1)}, f32[8,4,128,128]{3,2,1,0:T(8,128)}) custom-call(bf16[64,256]{1,0:T(8,128)(2,1)} %get-tuple-element.6.res_in, f32[8,4,128,128]{3,2,1,0:T(8,128)} %get-tuple-element.7.state_in), custom_call_target="tpu_custom_call" | custom-call | tf_op jit(solution)/shard_map/tail/pallas_call | solution.py:425

commit v7 on v6

--- a/solution.py
+++ b/solution.py
@@ -145,13 +145,16 @@
         sbuf[ch] = jnp.concatenate([part[:, :, :128], part[:, :, 128:]], axis=1).astype(BF16)
 
         def scatter(i, _, ch=ch):
-            zz, xx = zp(i // NX), xp(i % NX)
+            j, k = i // NX, i % NX
+            dz = lax.rem(4 + ((j + 1) // 2) * (1 - 2 * (j % 2)), NZ)
+            dx = lax.rem(2 + ((k + 1) // 2) * (1 - 2 * (k % 2)), NX)
+            zz, xx = zp(dz), xp(dx)
             remote(
-                sbuf.at[ch, zz * NX + xx], rbuf.at[ch, i], p1_ss.at[ch], p1_rs.at[ch], {"kv_0": zz, "kv_1": xx}
+                sbuf.at[ch, zz * NX + xx], rbuf.at[ch, dz * NX + dx], p1_ss.at[ch], p1_rs.at[ch], {"kv_0": zz, "kv_1": xx}
             )
             return 0
 
-        lax.fori_loop(1, NZ * NX, scatter, 0)
+        lax.fori_loop(0, NZ * NX - 1, scatter, 0)
 
     mlp_cp = [
         remote(w_up, wup.at[c], mlp_ss.at[0], mlp_rs.at[0], partner),

time: 75.6 us -> 75.2 us (level)
  no operation moved by 1% of the time
where the time goes in v7:
time: 75.2 us; the launch traced here: 75.1 us
  Pallas kernels  74.5 us (99%)
    pallas_call x1, Pallas kernels, per_device(): pl.pallas_call(kernel, out_shape=(jax.ShapeDtypeStruct((64, 256), BF16),...  72.1 us
    pallas_call x1, Pallas kernels, per_device(): pl.pallas_call(tail, out_shape=(jax.ShapeDtypeStruct((64, 256), BF16), ja...  2.41 us

profile of v7, /device:TPU:1, one launch (start us, length us, event | category | flops | bytes accessed | tf_op | source)
XLA Modules:
  0.0 75.1 jit_solution(487590855878589524)
XLA Ops:
  0.6 72.1 %layer.1 = (bf16[64,256]{1,0:T(8,128)(2,1)}, f32[8,4,128,128]{3,2,1,0:T(8,128)}) custom-call(bf16[64,256]{1,0:T(8,128)(2,1)} %bitcast.7, f32[1,4096]{1,0:T(1,128)} %bitcast.8, f32[1,4096]{1,0:T(1,128)} %bitcast.9, f32[16]{0:T(128)} %rates_h.1, bf16[128,512]{1,0:T(8,128)(2,1)} %w_query.1, bf16[128,512]{1,0:T(8,128)(2,1)} %w_key.1, bf16[128,1024]{1,0:T(8,128)(2,1)} %w_value.1, ...), custom_call_target="tpu_custom_call" | custom-call | tf_op jit(solution)/shard_map/layer/pallas_call | solution.py:373
  72.7 2.4 %tail.1 = (bf16[64,256]{1,0:T(8,128)(2,1)}, f32[8,4,128,128]{3,2,1,0:T(8,128)}) custom-call(bf16[64,256]{1,0:T(8,128)(2,1)} %get-tuple-element.6.res_in, f32[8,4,128,128]{3,2,1,0:T(8,128)} %get-tuple-element.7.state_in), custom_call_target="tpu_custom_call" | custom-call | tf_op jit(solution)/shard_map/tail/pallas_call | solution.py:428
